TPU v7x, 768 devices: a whole 4x8x12 slice. The times are simulated.
768 devices in a mesh: ep: 24 (over z, core), tp: 32 (over y, x).
Axes of the slice: x: 4, y: 8, z: 12, core: 2. Of those that a mesh axis runs over, the one named last changes fastest.
Arguments:
- tokens: bfloat16 [4032, 2048], P('ep', 'tp'), may hold values from -540 to 540
- norm_gain: float32 [2048], P('tp'), may hold values from 0.1 to 1.9
- chosen: int32 [24, 504], P('ep'), may hold values from 0 to 4031, as said below
- affinity: float32 [24, 504], P('ep'), may hold values from 0.1 to 1
- w_gate: bfloat16 [24, 2048, 8192], P('ep', None, 'tp'), may hold values from -0.125 to 0.125
- w_up: bfloat16 [24, 2048, 8192], P('ep', None, 'tp'), may hold values from -0.125 to 0.125
- w_down: bfloat16 [24, 8192, 2048], P('ep', 'tp'), may hold values from -0.0625 to 0.0625
Outputs:
- expert_mix: bfloat16 [4032, 2048], P('ep', 'tp')
Inputs may be any that keep to these rules, and one draw needn't show every extreme that they name: `chosen`: each expert's 504 token numbers are distinct. Among one expert's choices at most 42 are tokens of one index of ep, and that bound is reached in every draw.
All inputs are finite; a program needn't handle non-finite values.
Results may differ from a plain program's by a relative error of at most 0.025.
Values may be sent and summed in bfloat16 or wider, within the bound.
No kernel may reach another device: no remote copies, remote signals or barrier semaphores. Data moves between devices by JAX's collectives and lax.ppermute only.
A program may use at most 32 MiB of HBM per device.

v0:
```python
import jax
import jax.numpy as jnp
from jax import lax
from jax.sharding import PartitionSpec as P

D = 2048


EPS = 1e-06


def sent_to_all(array, axis):
    devices = lax.axis_size(axis)
    return lax.all_to_all(
        jnp.broadcast_to(array[None], (devices, *array.shape)), axis, 0, 0, tiled=True
    )


def of_everyone(array, axis):
    everything = sent_to_all(array, axis)
    return jnp.sum(everything, axis=0)


def laid_out(parts, dim):
    parts = jnp.moveaxis(parts, 0, dim)
    lengths = parts.shape
    return parts.reshape(*lengths[:dim], lengths[dim] * lengths[dim + 1], *lengths[dim + 2 :])


def gathered_copies(array, axis, dim):
    return laid_out(sent_to_all(array, axis), dim)


def split_up(array, dim, devices):
    lengths = array.shape
    parts = array.reshape(*lengths[:dim], devices, lengths[dim] // devices, *lengths[dim + 1 :])
    return jnp.moveaxis(parts, dim, 0)


def sum_at_owner(array, axis, dim):
    parts = split_up(array, dim, lax.axis_size(axis))
    arrived = lax.all_to_all(parts, axis, split_axis=0, concat_axis=0, tiled=True)
    return arrived.astype(jnp.float32).sum(axis=0)


def local(tokens, norm_gain, chosen, affinity, w_gate, w_up, w_down):
    tok_dev, width_part = tokens.shape
    ep_count = lax.axis_size("ep")
    floats = tokens.astype(jnp.float32)
    square_sum = of_everyone(jnp.sum(floats * floats, axis=1), "tp")
    normed = (floats * lax.rsqrt(square_sum / D + EPS)[:, None] * norm_gain[None, :]).astype(
        jnp.bfloat16
    )
    own_choice = chosen[0]
    chosen_count = own_choice.shape[0]
    bound_rows = min(tok_dev, 2 * chosen_count // ep_count)
    slot_ids = jnp.arange(bound_rows, dtype=jnp.int32)
    positions = jnp.arange(chosen_count, dtype=jnp.int32)
    every_token = gathered_copies(normed, "ep", 0)
    picked = every_token[own_choice]
    piece = gathered_copies(picked, "tp", 1)
    gate_rows = w_gate[0]
    up_rows = w_up[0]
    gate = jnp.dot(piece, gate_rows, preferred_element_type=jnp.float32)
    upward = jnp.dot(piece, up_rows, preferred_element_type=jnp.float32)
    hidden = (jax.nn.silu(gate) * upward).astype(jnp.bfloat16)
    columns = w_down[0]
    summed = sum_at_owner(
        lax.dot_general(
            columns, hidden, (((0,), (1,)), ((), ())), preferred_element_type=jnp.float32
        ).astype(jnp.bfloat16),
        "tp",
        0,
    )
    weighted = (summed * affinity[0][None, :]).astype(jnp.bfloat16).T
    owner = own_choice // tok_dev
    owner_local = own_choice - owner * tok_dev
    owner_hot = owner[:, None] == jnp.arange(ep_count, dtype=jnp.int32)[None, :]
    running = jnp.cumsum(owner_hot.astype(jnp.int32), axis=0)
    place = jnp.sum(jnp.where(owner_hot, running, 0), axis=1) - 1
    back_match = owner_hot.T[:, None, :] & (place[None, None, :] == slot_ids[None, :, None])
    back_filled = jnp.any(back_match, axis=2)
    back_pick = jnp.sum(jnp.where(back_match, positions[None, None, :], 0), axis=2)
    back_rows = jnp.where(back_filled[..., None], weighted[back_pick], jnp.zeros((), jnp.bfloat16))
    back_token = jnp.where(back_filled, owner_local[back_pick], tok_dev)
    got_back, got_token = (
        lax.all_to_all(back_rows, "ep", split_axis=0, concat_axis=0, tiled=True),
        lax.all_to_all(back_token, "ep", split_axis=0, concat_axis=0, tiled=True),
    )
    total = jnp.zeros((tok_dev, width_part), jnp.float32)
    total = total.at[got_token.reshape(-1)].add(
        got_back.reshape(-1, width_part).astype(jnp.float32), mode="drop"
    )
    return total.astype(jnp.bfloat16)


def solution(mesh):
    in_specs = (
        P("ep", "tp"),
        P("tp"),
        P("ep", None),
        P("ep", None),
        P("ep", None, "tp"),
        P("ep", None, "tp"),
        P("ep", "tp", None),
    )
    out_specs = P("ep", "tp")
    return jax.shard_map(local, mesh=mesh, in_specs=in_specs, out_specs=out_specs, check_vma=False)
```

profile of v0, /device:TPU:1, one launch (start us, length us, event | category | flops | bytes accessed | tf_op | source)
XLA Modules:
  0.0 232.7 jit_solution(17342360270769848611)
XLA Ops:
  0.0 0.9 fusion.14
  0.9 19.0 %all_to_all.32 = f32[32,1,168]{2,1,0:T(1,128)S(1)} all-to-all(f32[32,1,168]{2,1,0:T(1,128)S(1)} %broadcast_in_dim.72), channel_id=1, replica_groups=mesh['ep'=24,'tp'=32] {'tp'}, dimensions={0} | all-to-all | bytes 43008 | tf_op jit(solution)/shard_map/all_to_all | solution.py:14
  19.9 0.1 reduce_sum.51
  20.0 0.8 fusion.16
  20.8 1.0 broadcast_in_dim.73
  21.8 17.3 %all-to-all-start.2 = ((bf16[24,168,64]{1,2,0:T(8,128)(2,1)}), bf16[24,168,64]{1,2,0:T(8,128)(2,1)S(1)}, u32[]{:S(2)}, u32[]{:S(2)}) async-start(bf16[24,168,64]{1,2,0:T(8,128)(2,1)} %broadcast_in_dim.73), calls=%async_computation.2 | async-start | bytes 1572864 | tf_op jit(solution)/shard_map/all_to_all | solution.py:14
  39.1 30.7 %all-to-all-done.2 = bf16[24,168,64]{1,2,0:T(8,128)(2,1)S(1)} async-done(((bf16[24,168,64]{1,2,0:T(8,128)(2,1)}), bf16[24,168,64]{1,2,0:T(8,128)(2,1)S(1)}, u32[]{:S(2)}, u32[]{:S(2)}) %all-to-all-start.2) | async-done | bytes 516128 | tf_op jit(solution)/shard_map/all_to_all | solution.py:14
  69.9 0.7 copy.80
  70.5 1.5 gather_fusion.1
  72.1 0.1 copy.81
  72.2 0.2 broadcast_in_dim.74
  72.4 50.3 %all_to_all.33 = bf16[32,504,64]{1,2,0:T(8,128)(2,1)S(1)} all-to-all(bf16[32,504,64]{1,2,0:T(8,128)(2,1)S(1)} %broadcast_in_dim.74), channel_id=1, replica_groups=mesh['ep'=24,'tp'=32] {'tp'}, dimensions={0} | all-to-all | bytes 4128768 | tf_op jit(solution)/shard_map/all_to_all | solution.py:14
  122.7 1.5 fusion.6
  124.2 4.9 %fusion = bf16[2048,504]{0,1:T(8,128)(2,1)} fusion(bf16[504,2048]{0,1:T(8,128)(2,1)S(1)} %bitcast.48, bf16[1,256,2048]{2,1,0:T(8,128)(2,1)S(1)} %copy-done, bf16[1,2048,256]{2,1,0:T(8,128)(2,1)} %param.12, f32[504,256]{1,0:T(8,128)} %fusion.6), kind=kOutput, calls=%fused_computation.6 | convolution fusion | flops 1058770944 | bytes 6742016 | tf_op jit(solution)/shard_map/dot_general | solution.py:69
  129.2 3.9 %copy.82 = bf16[2048,504]{1,0:T(8,128)(2,1)} copy(bf16[2048,504]{0,1:T(8,128)(2,1)} %fusion) | data formatting | bytes 4128768 | tf_op jit(solution)/shard_map/convert_element_type | solution.py:71
  133.1 7.4 %all-to-all-start.4 = ((bf16[32,64,504]{2,1,0:T(8,128)(2,1)}), bf16[32,64,504]{2,1,0:T(8,128)(2,1)S(1)}, u32[]{:S(2)}, u32[]{:S(2)}) async-start(bf16[32,64,504]{2,1,0:T(8,128)(2,1)} %bitcast.49), calls=%async_computation.4 | async-start | bytes 4194304 | tf_op jit(solution)/shard_map/all_to_all | solution.py:42
  140.5 1.2 reduce-window.6
  141.7 0.2 slice_reduce_fusion
  142.0 0.1 bitcast_bitcast_fusion
  142.1 0.8 fusion.1
  142.9 0.1 copy.75
  143.0 0.1 reshape.199
  143.1 0.8 and_reduce_fusion
  143.9 0.1 copy.78
  144.0 6.9 %gather_fusion = s32[1008]{0:T(1024)S(1)} fusion(s32[504]{0:T(512)S(1)} %get-tuple-element.5, s32[1024]{0:T(1024)S(1)} %pad_clamp_fusion.1), kind=kCustom, calls=%fused_computation | custom fusion | bytes 12096 | tf_op jit(solution)/shard_map/gather | solution.py:85
  150.9 0.1 reshape.198
  151.0 0.1 copy.76
  151.1 0.7 copy.77
  151.8 34.9 %all-to-all-done.4 = bf16[32,64,504]{2,1,0:T(8,128)(2,1)S(1)} async-done(((bf16[32,64,504]{2,1,0:T(8,128)(2,1)}), bf16[32,64,504]{2,1,0:T(8,128)(2,1)S(1)}, u32[]{:S(2)}, u32[]{:S(2)}) %all-to-all-start.4) | async-done | bytes 2064416 | tf_op jit(solution)/shard_map/all_to_all | solution.py:42
  186.7 11.5 %all-to-all-start = ((s32[24,1,42]{2,1,0:T(1,128)}), s32[24,1,42]{2,1,0:T(1,128)S(1)}, u32[]{:S(2)}, u32[]{:S(2)}) async-start(s32[24,1,42]{2,1,0:T(1,128)} %copy.77), calls=%async_computation | async-start | bytes 24576 | tf_op jit(solution)/shard_map/all_to_all | solution.py:88
  198.2 0.3 convert_reduce_fusion
  198.6 0.2 copy.83
  198.7 3.3 %gather_fusion.2 = bf16[1008,64]{1,0:T(8,128)(2,1)S(1)} fusion(bf16[504,64]{1,0:T(8,128)(2,1)S(1)} %copy.83, s32[1024]{0:T(1024)S(1)} %pad_clamp_fusion.1), kind=kCustom, calls=%fused_computation.2 | custom fusion | bytes 262080 | tf_op jit(solution)/shard_map/gather | solution.py:84
  202.1 0.1 copy.84
  202.2 0.4 reshape.214
  202.6 0.3 copy.85
  203.0 0.9 reshape.244
  203.8 3.7 %all-to-all-done = s32[24,1,42]{2,1,0:T(1,128)S(1)} async-done(((s32[24,1,42]{2,1,0:T(1,128)}), s32[24,1,42]{2,1,0:T(1,128)S(1)}, u32[]{:S(2)}, u32[]{:S(2)}) %all-to-all-start) | async-done | bytes 4064 | tf_op jit(solution)/shard_map/all_to_all | solution.py:88
  207.6 6.0 %all-to-all-start.5 = ((bf16[24,2,1344]{2,1,0:T(2,128)(2,1)}), bf16[24,2,1344]{2,1,0:T(2,128)(2,1)S(1)}, u32[]{:S(2)}, u32[]{:S(2)}) async-start(bf16[24,2,1344]{2,1,0:T(2,128)(2,1)} %reshape.244), calls=%async_computation.5 | async-start | bytes 270336 | tf_op jit(solution)/shard_map/all_to_all | solution.py:87
  213.5 0.5 broadcast.166
  214.1 0.7 reduce.6
  214.7 0.1 reshape.191
  214.9 10.6 %all-to-all-done.5 = bf16[24,2,1344]{2,1,0:T(2,128)(2,1)S(1)} async-done(((bf16[24,2,1344]{2,1,0:T(2,128)(2,1)}), bf16[24,2,1344]{2,1,0:T(2,128)(2,1)S(1)}, u32[]{:S(2)}, u32[]{:S(2)}) %all-to-all-start.5) | async-done | bytes 129056 | tf_op jit(solution)/shard_map/all_to_all | solution.py:87
  225.4 0.3 reshape.245
  225.7 0.1 copy_convert_fusion
  225.8 0.1 copy.90
  225.9 6.0 %scatter_custom_fusion = f32[168,64]{1,0:T(8,128)S(1)} fusion(s32[1008]{0:T(1024)S(1)} %bitcast.53, f32[1008,64]{1,0:T(8,128)S(1)} %reshape.231, f32[]{:T(128)} %constant.12.clone.1), kind=kCustom, calls=%fused_computation.42 | custom fusion | flops 64512 | bytes 43012 | tf_op jit(solution)/shard_map/scatter-add | solution.py:91
  232.0 0.7 copy.89
  (27 shorter events, 0.3 us)
Async XLA Ops:
  0.0 124.2 %copy-start = (bf16[1,256,2048]{2,1,0:T(8,128)(2,1)S(1)}, bf16[1,256,2048]{2,1,0:T(8,128)(2,1)}, u32[]{:S(2)}) copy-start(bf16[1,256,2048]{2,1,0:T(8,128)(2,1)} %param.13) | copy-start | bytes 3145732
  0.0 39.1 %copy-start.2 = (s32[1,504]{1,0:T(1,128)S(1)}, s32[1,504]{1,0:T(1,128)}, u32[]{:S(2)}) copy-start(s32[1,504]{1,0:T(1,128)} %param.9) | copy-start | bytes 6052
  21.8 48.1 %all-to-all-start.2 = ((bf16[24,168,64]{1,2,0:T(8,128)(2,1)}), bf16[24,168,64]{1,2,0:T(8,128)(2,1)S(1)}, u32[]{:S(2)}, u32[]{:S(2)}) async-start(bf16[24,168,64]{1,2,0:T(8,128)(2,1)} %broadcast_in_dim.73), calls=%async_computation.2 | async-start | bytes 1572864 | tf_op jit(solution)/shard_map/all_to_all | solution.py:14
  72.4 50.3 %copy-start.1 = (bf16[1,2048,256]{2,1,0:T(8,128)(2,1)S(1)}, bf16[1,2048,256]{2,1,0:T(8,128)(2,1)}, u32[]{:S(2)}) copy-start(bf16[1,2048,256]{2,1,0:T(8,128)(2,1)} %param.11) | copy-start | bytes 3145732
  133.1 53.6 %all-to-all-start.4 = ((bf16[32,64,504]{2,1,0:T(8,128)(2,1)}), bf16[32,64,504]{2,1,0:T(8,128)(2,1)S(1)}, u32[]{:S(2)}, u32[]{:S(2)}) async-start(bf16[32,64,504]{2,1,0:T(8,128)(2,1)} %bitcast.49), calls=%async_computation.4 | async-start | bytes 4194304 | tf_op jit(solution)/shard_map/all_to_all | solution.py:42
  150.9 47.6 %copy-start.3 = (f32[1,504]{1,0:T(1,128)S(1)}, f32[1,504]{1,0:T(1,128)}, u32[]{:S(2)}) copy-start(f32[1,504]{1,0:T(1,128)} %param.10) | copy-start | bytes 6052
  186.7 20.9 %all-to-all-start = ((s32[24,1,42]{2,1,0:T(1,128)}), s32[24,1,42]{2,1,0:T(1,128)S(1)}, u32[]{:S(2)}, u32[]{:S(2)}) async-start(s32[24,1,42]{2,1,0:T(1,128)} %copy.77), calls=%async_computation | async-start | bytes 24576 | tf_op jit(solution)/shard_map/all_to_all | solution.py:88
  207.6 17.9 %all-to-all-start.5 = ((bf16[24,2,1344]{2,1,0:T(2,128)(2,1)}), bf16[24,2,1344]{2,1,0:T(2,128)(2,1)S(1)}, u32[]{:S(2)}, u32[]{:S(2)}) async-start(bf16[24,2,1344]{2,1,0:T(2,128)(2,1)} %reshape.244), calls=%async_computation.5 | async-start | bytes 270336 | tf_op jit(solution)/shard_map/all_to_all | solution.py:87
where the time goes:
time: 233 us
  waiting for transfers between devices  80 us (34%)
  blocking collectives  69.3 us (30%)
  starting transfers between devices  42.1 us (18%)
  local copies, waits for them, and re-layouts  22.6 us (10%)
  other arithmetic  11.9 us (5%)
  matrix products  6.47 us (3%)
    all_to_all x2, blocking collectives, sent_to_all(): lax.all_to_all(jnp.broadcast_to(array[None], (devices, *array.shape)), ax...  69.3 us
    all_to_all x1, waiting for transfers between devices, sum_at_owner(): lax.all_to_all(parts, axis, split_axis=0, concat_axis=0, tiled=True)  34.9 us
    all_to_all x1, waiting for transfers between devices, sent_to_all(): lax.all_to_all(jnp.broadcast_to(array[None], (devices, *array.shape)), ax...  30.7 us
    all_to_all x1, starting transfers between devices, sent_to_all(): lax.all_to_all(jnp.broadcast_to(array[None], (devices, *array.shape)), ax...  17.3 us
    all_to_all x1, starting transfers between devices, local(): lax.all_to_all(back_token, 'ep', split_axis=0, concat_axis=0, tiled=True)  11.5 us
    all_to_all x1, waiting for transfers between devices, local(): lax.all_to_all(back_rows, 'ep', split_axis=0, concat_axis=0, tiled=True)  10.6 us
    all_to_all x1, starting transfers between devices, sum_at_owner(): lax.all_to_all(parts, axis, split_axis=0, concat_axis=0, tiled=True)  7.36 us
    gather x3, local copies, waits for them, and re-layouts, local(): back_token = jnp.where(back_filled, owner_local[back_pick], tok_dev)  7.04 us
  transfers between devices with their start and end apart: 4, of which 4 were waited for; matrix products, arithmetic and copies ran while one was open for 8% of the time, Pallas kernels for 0%

commit v1 on v0

v1 whole, which is shorter than its diff:
```python
import functools

import jax
import jax.numpy as jnp
from jax import lax
from jax.experimental import pallas as pl
from jax.experimental.pallas import tpu as pltpu
from jax.sharding import Mesh, PartitionSpec as P


EPS = 1e-06
SLOTS = 512
VMEM = pl.BlockSpec(memory_space=pltpu.VMEM)
SMEM = pl.BlockSpec(memory_space=pltpu.SMEM)
BF16 = jnp.bfloat16
F32 = jnp.float32
PLANE = ("core", "y", "x")


def call(kernel, outs, args, specs=None, scratch=(), flops=0, vmem=16):
    return pl.pallas_call(
        kernel,
        out_shape=outs,
        in_specs=specs or [VMEM] * len(args),
        out_specs=jax.tree.map(lambda _: VMEM, outs),
        scratch_shapes=list(scratch),
        compiler_params=pltpu.CompilerParams(vmem_limit_bytes=vmem * 1024 * 1024),
        cost_estimate=pl.CostEstimate(flops=flops, bytes_accessed=0, transcendentals=0),
    )(*args)


def place(core, y, x, ny, nx):
    return ((y + core) % ny) * nx + (x + core) % nx


def tiles(ny, nx):
    near, far = [], []
    for c in range(2):
        base = c * ny * nx

        def at(Y, X, b, a, c=c, base=base):
            return base + place(c, 2 * Y + b, 2 * X + a, ny, nx)

        corners = [(b, a) for b in range(2) for a in range(2)]
        cells = [(Y, X) for Y in range(ny // 2) for X in range(nx // 2)]
        near += [[at(Y, X, b, a) for b, a in corners] for Y, X in cells]
        far += [[at(Y, X, b, a) for Y, X in cells] for b, a in corners]
    return near, far


def to_all(array, axis, groups=None):
    n = len(groups[0]) if groups else lax.axis_size(axis)
    return lax.all_to_all(
        jnp.broadcast_to(array[None], (n, *array.shape)),
        axis,
        0,
        0,
        axis_index_groups=groups,
        tiled=True,
    )


def hot(ids, base, rows):
    row = lax.broadcasted_iota(jnp.int32, (rows, ids.shape[1]), 0)
    return jnp.where(row == ids - base, 1.0, 0.0).astype(BF16)


def pick_kernel(core_ref, gathered, own_ref, sib_ref, gain, mine, other):
    blocks, _, rows = gathered.shape
    core = core_ref[0]
    acc = jnp.zeros(mine.shape, F32)
    acc2 = jnp.zeros(mine.shape, F32)
    for b in range(blocks):
        base = (2 * b + core) * rows
        acc += jnp.dot(gathered[b], hot(own_ref[...], base, rows), preferred_element_type=F32)
        acc2 += jnp.dot(gathered[b], hot(sib_ref[...], base, rows), preferred_element_type=F32)
    high = gain[...].astype(BF16)
    rest = gain[...] - high.astype(F32)
    middle = rest.astype(BF16)
    low = (rest - middle.astype(F32)).astype(BF16)
    lane = lax.broadcasted_iota(jnp.int32, mine.shape, 1)
    first = SLOTS - 8
    acc = jnp.where(lane == first, high.astype(F32), acc)
    acc = jnp.where(lane == first + 1, middle.astype(F32), acc)
    acc = jnp.where(lane == first + 2, low.astype(F32), acc)
    mine[...] = acc.astype(BF16)
    other[...] = acc2.astype(BF16)


def block_of(core, corner, cell, ny, nx):
    Y, X = cell // (nx // 2), cell % (nx // 2)
    b, a = corner // 2, corner % 2
    return place(core, 2 * Y + b, 2 * X + a, ny, nx)


def turn_kernel(ny, nx, core_ref, gate_ref, up_ref, out):
    _, _, hid = gate_ref.shape
    cells = ny * nx // 4
    for s in range(4):
        for half, ref in enumerate((gate_ref, up_ref)):
            pieces = [ref[block_of(core_ref[0], s, g, ny, nx)] for g in range(cells)]
            rows = jnp.concatenate(pieces, axis=0)
            out[s, half * hid : (half + 1) * hid] = rows.T


def turn_down_kernel(ny, nx, core_ref, down_ref, out, turned):
    corners, cells, part, hid = out.shape
    for y in range(ny):
        rows = down_ref[:, y * nx * part : (y + 1) * nx * part].T
        turned[y * nx : (y + 1) * nx] = rows.reshape(nx, part, hid)
    for s in range(corners):
        for g in range(cells):
            out[s, g] = turned[block_of(core_ref[0], s, g, ny, nx)]


def hidden_kernel(x_ref, w_ref, out, normed):
    corners, depth, slots = x_ref.shape
    hid = out.shape[0]
    width = corners * depth
    square = jnp.zeros((1, slots), F32)
    for s in range(corners):
        v = x_ref[s].astype(F32)
        square += jnp.sum(v * v, axis=0, keepdims=True)
    scale = lax.rsqrt(square / width + EPS)
    acc = jnp.zeros((2 * hid, slots), F32)
    for s in range(corners):
        v = x_ref[s]
        parts = v[:, slots - 128 :].astype(F32)
        lane = lax.broadcasted_iota(jnp.int32, parts.shape, 1)
        keep = (lane >= 120) & (lane < 123)
        gain = jnp.sum(jnp.where(keep, parts, 0.0), axis=1, keepdims=True)
        normed[...] = (v.astype(F32) * scale * gain).astype(BF16)
        acc += jnp.dot(w_ref[s], normed[...], preferred_element_type=F32)
    gate, up = acc[:hid], acc[hid:]
    out[...] = (gate / (1.0 + jnp.exp(-gate)) * up).astype(BF16)


def down_kernel(corner_ref, hidden, w0, w1, w2, w3, out):
    me = corner_ref[0]
    acc = jnp.zeros(out.shape, F32)
    for flip, w in enumerate((w0, w1, w2, w3)):
        acc += jnp.dot(w[...], hidden[me ^ flip], preferred_element_type=F32)
    out[...] = acc.astype(BF16)


def spread_kernel(core_ref, mine, other, own_ref, sib_ref, out):
    blocks, _, rows = out.shape
    core = core_ref[0]
    dims = (((1,), (1,)), ((), ()))
    for b in range(blocks):
        base = (2 * b + core) * rows
        total = lax.dot_general(
            mine[...], hot(own_ref[...], base, rows), dims, preferred_element_type=F32
        )
        total += lax.dot_general(
            other[...], hot(sib_ref[...], base, rows), dims, preferred_element_type=F32
        )
        out[b] = total.astype(BF16)


def local(tokens, norm_gain, chosen, affinity, w_gate, w_up, w_down):
    tok_dev, part = tokens.shape
    nz, ny, nx = lax.axis_size("z"), lax.axis_size("y"), lax.axis_size("x")
    width, hid = w_gate.shape[1:]
    tp, cells = ny * nx, ny * nx // 4
    near, far = tiles(ny, nx)
    count = chosen.shape[1]
    swap = [(0, 1), (1, 0)]
    core_index = lax.axis_index("core").astype(jnp.int32)
    y_index = lax.axis_index("y").astype(jnp.int32)
    x_index = lax.axis_index("x").astype(jnp.int32)
    corner_index = ((y_index + core_index) & 1) * 2 + ((x_index + core_index) & 1)
    core, corner = core_index.reshape(1), corner_index.reshape(1)

    gathered = to_all(tokens.T, "z")

    own_ids = jnp.pad(chosen, ((0, 0), (0, SLOTS - count)), constant_values=-1)
    sib_ids = lax.ppermute(own_ids, "core", swap)
    down_blocks = call(
        functools.partial(turn_down_kernel, ny, nx),
        jax.ShapeDtypeStruct((4, cells, part, hid), BF16),
        (core, w_down[0]),
        [SMEM, VMEM],
        [pltpu.VMEM((tp, part, hid), BF16)],
        flops=1 << 30,
    ).reshape(4, cells * part, hid)
    downs = [lax.dynamic_index_in_dim(down_blocks, corner_index, 0, False)]
    for flip in range(1, 4):
        block = lax.dynamic_index_in_dim(down_blocks, corner_index ^ flip, 0, False)
        pairs = [(g[s], g[s ^ flip]) for g in near for s in range(4)]
        downs.append(lax.ppermute(block, PLANE, pairs))
    turned = call(
        functools.partial(turn_kernel, ny, nx),
        jax.ShapeDtypeStruct((4, 2 * hid, cells * part), BF16),
        (core, w_gate[0].reshape(tp, part, hid), w_up[0].reshape(tp, part, hid)),
        [SMEM, VMEM, VMEM],
        flops=1 << 30,
    )
    gathered, downs, turned = lax.optimization_barrier((gathered, downs, turned))

    slots = jax.ShapeDtypeStruct((part, SLOTS), BF16)
    own, other = call(
        pick_kernel,
        [slots, slots],
        (core, gathered, own_ids, sib_ids, norm_gain[:, None]),
        [SMEM] + [VMEM] * 4,
        flops=4 * part * nz * tok_dev * SLOTS,
    )
    picked = own + lax.ppermute(other, "core", swap)

    column = to_all(picked, PLANE, far).reshape(cells * part, SLOTS)
    full = to_all(column, PLANE, near)
    hidden = call(
        hidden_kernel,
        jax.ShapeDtypeStruct((hid, SLOTS), BF16),
        (full, turned),
        scratch=[pltpu.VMEM((cells * part, SLOTS), BF16)],
        flops=4 * width * hid * SLOTS,
    )
    tile_hidden = to_all(hidden, PLANE, near)
    partial = call(
        down_kernel,
        jax.ShapeDtypeStruct((cells * part, SLOTS), BF16),
        (corner, tile_hidden, *downs),
        [SMEM] + [VMEM] * 5,
        flops=2 * width * hid * SLOTS,
    )
    arrived = lax.all_to_all(
        partial.reshape(cells, part, SLOTS), PLANE, 0, 0, axis_index_groups=far, tiled=True
    )
    weight = jnp.pad(affinity, ((0, 0), (0, SLOTS - count)))
    weighted = (jnp.sum(arrived.astype(F32), axis=0) * weight).astype(BF16)
    weighted_other = lax.ppermute(weighted, "core", swap)
    dense = call(
        spread_kernel,
        jax.ShapeDtypeStruct((nz, part, tok_dev), BF16),
        (core, weighted, weighted_other, own_ids, sib_ids),
        [SMEM] + [VMEM] * 4,
        flops=4 * part * nz * tok_dev * SLOTS,
    )
    back = lax.all_to_all(dense, "z", 0, 0, tiled=True)
    return jnp.sum(back.astype(F32), axis=0).astype(BF16).T


def solution(mesh):
    nz, ny, nx = 12, 8, 4
    fine = Mesh(mesh.devices.reshape(nz, 2, ny, nx), ("z", "core", "y", "x"))
    ep, tp = ("z", "core"), ("y", "x")
    in_specs = (
        P(ep, tp),
        P(tp),
        P(ep, None),
        P(ep, None),
        P(ep, None, tp),
        P(ep, None, tp),
        P(ep, tp, None),
    )

    return jax.shard_map(local, mesh=fine, in_specs=in_specs, out_specs=P(ep, tp), check_vma=False)
```

time: 233 us -> 158 us (0.68)
  waiting for transfers between devices: 80 us -> 21.4 us
  local copies, waits for them, and re-layouts: 22.6 us -> 5.48 us
  other arithmetic: 11.9 us -> 0.79 us
  blocking collectives: 69.3 us -> 78.9 us
  matrix products: 6.47 us -> 0 us
  Pallas kernels: 0 us -> 6.4 us
    all_to_all x4 -> x2, waiting for transfers between devices: 80 us -> 13.9 us  [the longest x1 13.9 us: local(): lax.all_to_all(partial.reshape(cells, part, SLOTS), PLANE, 0, 0, axis_ind...]
    all_to_all x4 -> x2, starting transfers between devices: 42.1 us -> 24.1 us  [the longest x1 15.7 us: to_all(): lax.all_to_all(jnp.broadcast_to(array[None], (n, *array.shape)), axis, 0,...]
    ppermute x0 -> x6, starting transfers between devices: none -> 18.1 us  [the longest x3 11.4 us: local(): downs.append(lax.ppermute(block, PLANE, pairs))]
    gather x8 -> x0, local copies, waits for them, and re-layouts: 12.5 us -> none  [the longest x3 7.04 us: local(): back_token = jnp.where(back_filled, owner_local[back_pick], tok_dev)]
    all_to_all x2 -> x4, blocking collectives: 69.3 us -> 78.9 us  [the longest x3 53.9 us: to_all(): lax.all_to_all(jnp.broadcast_to(array[None], (n, *array.shape)), axis, 0,...]
    ppermute x0 -> x6, waiting for transfers between devices: none -> 7.48 us  [the longest x3 5.38 us: local(): downs.append(lax.ppermute(block, PLANE, pairs))]
    dot_general x2 -> x0, matrix products: 6.47 us -> none  [the longest x1 4.94 us: local(): lax.dot_general(columns, hidden, (((0,), (1,)), ((), ())), preferred_elem...]
    pallas_call x0 -> x6, Pallas kernels: none -> 6.4 us  [call(): pl.pallas_call(kernel, out_shape=outs, in_specs=specs or [VMEM] * len(arg...]
  transfers between devices with their start and end apart: 4 -> 8, of which waited for: 4 -> 4; matrix products, arithmetic and copies ran while one was open for 8% -> 1% of each run, Pallas kernels for 0% -> 1%
where the time goes in v1:
time: 158 us; the launch traced here: 155 us
  blocking collectives  78.9 us (50%)
  starting transfers between devices  42.1 us (27%)
  waiting for transfers between devices  21.4 us (14%)
  Pallas kernels  6.4 us (4%)
  local copies, waits for them, and re-layouts  5.48 us (3%)
    all_to_all x3, blocking collectives, to_all(): lax.all_to_all(jnp.broadcast_to(array[None], (n, *array.shape)), axis, 0,...  53.9 us
    all_to_all x1, blocking collectives, local(): back = lax.all_to_all(dense, 'z', 0, 0, tiled=True)  25 us
    all_to_all x1, starting transfers between devices, to_all(): lax.all_to_all(jnp.broadcast_to(array[None], (n, *array.shape)), axis, 0,...  15.7 us
    all_to_all x1, waiting for transfers between devices, local(): lax.all_to_all(partial.reshape(cells, part, SLOTS), PLANE, 0, 0, axis_ind...  13.9 us
    ppermute x3, starting transfers between devices, local(): downs.append(lax.ppermute(block, PLANE, pairs))  11.4 us
    all_to_all x1, starting transfers between devices, local(): lax.all_to_all(partial.reshape(cells, part, SLOTS), PLANE, 0, 0, axis_ind...  8.37 us
    pallas_call x6, Pallas kernels, call(): pl.pallas_call(kernel, out_shape=outs, in_specs=specs or [VMEM] * len(arg...  6.4 us
    ppermute x3, waiting for transfers between devices, local(): downs.append(lax.ppermute(block, PLANE, pairs))  5.38 us
  transfers between devices with their start and end apart: 8, of which 4 were waited for; matrix products, arithmetic and copies ran while one was open for 1% of the time, Pallas kernels for 1%

profile of v1, /device:TPU:1, one launch (start us, length us, event | category | flops | bytes accessed | tf_op | source)
XLA Modules:
  0.0 155.4 jit_solution(8170401856453253329)
XLA Ops:
  0.0 1.5 broadcast_in_dim.12
  1.5 15.7 %all-to-all-start = ((bf16[12,64,168]{2,1,0:T(8,128)(2,1)}), bf16[12,64,168]{2,1,0:T(8,128)(2,1)S(1)}, u32[]{:S(2)}, u32[]{:S(2)}) async-start(bf16[12,64,168]{2,1,0:T(8,128)(2,1)} %broadcast_in_dim.12), calls=%async_computation | async-start | bytes 786432 | tf_op jit(solution)/shard_map/all_to_all | solution.py:53
  17.3 0.0 copy-start.3
  17.3 1.2 copy-done.3
  18.5 0.0 copy-start.4
  18.5 0.0 copy-start
  18.5 0.0 copy-start.1
  18.5 0.4 shard_map.73
  18.9 0.9 dynamic-slice_bitcast_fusion
  19.8 4.4 %collective-permute-start = (bf16[512,256]{1,0:T(8,128)(2,1)}, bf16[512,256]{1,0:T(8,128)(2,1)S(1)}, u32[]{:S(2)}, u32[]{:S(2)}) collective-permute-start(bf16[512,256]{1,0:T(8,128)(2,1)} %get-tuple-element.23), channel_id=1, source_target_pairs={{0,1},{1,0},{4,5},{5,4},{2,3},{3,2},{6,7},{7,6},{8,9},{9,8},{12,13... | collective-permute-start | bytes 786440 | tf_op jit(solution)/shard_map/ppermute | solution.py:191
  24.2 5.1 %collective-permute-start.1 = (bf16[512,256]{1,0:T(8,128)(2,1)}, bf16[512,256]{1,0:T(8,128)(2,1)S(1)}, u32[]{:S(2)}, u32[]{:S(2)}) collective-permute-start(bf16[512,256]{1,0:T(8,128)(2,1)} %get-tuple-element.22), channel_id=1, source_target_pairs={{0,4},{1,5},{4,0},{5,1},{2,6},{3,7},{6,2},{7,3},{8,12},{9,13},{12,... | collective-permute-start | bytes 786440 | tf_op jit(solution)/shard_map/ppermute | solution.py:191
  29.3 1.9 %collective-permute-start.2 = (bf16[512,256]{1,0:T(8,128)(2,1)}, bf16[512,256]{1,0:T(8,128)(2,1)S(1)}, u32[]{:S(2)}, u32[]{:S(2)}) collective-permute-start(bf16[512,256]{1,0:T(8,128)(2,1)} %get-tuple-element.21), channel_id=1, source_target_pairs={{0,5},{1,4},{4,1},{5,0},{2,7},{3,6},{6,3},{7,2},{8,13},{9,12},{12,... | collective-permute-start | bytes 786440 | tf_op jit(solution)/shard_map/ppermute | solution.py:191
  31.2 0.0 copy-done.4
  31.2 1.9 %collective-permute-start.3 = (s32[1,512]{1,0:T(1,128)S(1)}, s32[1,512]{1,0:T(1,128)S(1)}, u32[]{:S(2)}, u32[]{:S(2)}) collective-permute-start(s32[1,512]{1,0:T(1,128)S(1)} %pad.8.own_ref), channel_id=1, source_target_pairs={{0,32},{32,0},{1,33},{33,1},{2,34},{34,2},{3,35},{35,3},{4,36},{36... | collective-permute-start | bytes 6152 | tf_op jit(solution)/shard_map/ppermute | solution.py:178
  33.2 0.0 copy-done
  33.2 0.0 copy-done.1
  33.2 0.0 copy-start.6
  33.2 0.6 shard_map.74.w_ref
  33.8 0.0 copy-done.6
  33.9 0.7 copy.8.gain
  34.6 0.0 collective-permute-done.w1
  34.6 0.0 collective-permute-done.1.w2
  34.6 5.4 %collective-permute-done.2.w3 = bf16[512,256]{1,0:T(8,128)(2,1)S(1)} collective-permute-done((bf16[512,256]{1,0:T(8,128)(2,1)}, bf16[512,256]{1,0:T(8,128)(2,1)S(1)}, u32[]{:S(2)}, u32[]{:S(2)}) %collective-permute-start.2) | collective-permute-done | bytes 262176 | tf_op jit(solution)/shard_map/ppermute | solution.py:191
  39.9 0.0 all-to-all-done.gathered
  39.9 0.0 collective-permute-done.3.sib_ref
  39.9 0.0 copy-start.2
  40.0 0.8 copy-done.2
  40.7 1.0 shard_map.75
  41.7 1.9 %collective-permute-start.4 = (bf16[64,512]{1,0:T(8,128)(2,1)S(1)}, bf16[64,512]{1,0:T(8,128)(2,1)S(1)}, u32[]{:S(2)}, u32[]{:S(2)}) collective-permute-start(bf16[64,512]{1,0:T(8,128)(2,1)S(1)} %get-tuple-element.15), channel_id=1, source_target_pairs={{0,32},{32,0},{1,33},{33,1},{2,34},{34,2},{3,35},{35,3},{4,36},{36... | collective-permute-start | bytes 196616 | tf_op jit(solution)/shard_map/ppermute | solution.py:209
  43.6 1.2 collective-permute-done.4
  44.9 21.4 %all_to_all.30 = bf16[8,64,512]{2,1,0:T(8,128)(2,1)S(1)} all-to-all(bf16[8,64,512]{2,1,0:T(8,128)(2,1)S(1)} %broadcast_in_dim.14), channel_id=1, replica_groups={{0,2,8,10,16,18,24,26},{1,3,9,11,17,19,25,27},{4,6,12,14,20,22,28,30},{..., dimensions={0} | all-to-all | bytes 1048576 | tf_op jit(solution)/shard_map/all_to_all | solution.py:53
  66.3 0.2 broadcast_in_dim.32
  66.5 19.0 %all_to_all.31.x_ref = bf16[4,512,512]{2,1,0:T(8,128)(2,1)S(1)} all-to-all(bf16[4,512,512]{2,1,0:T(8,128)(2,1)S(1)} %broadcast_in_dim.32), channel_id=1, replica_groups={{0,1,4,5},{2,3,6,7},{8,9,12,13},{10,11,14,15},{16,17,20,21},{18,19,22,2..., dimensions={0} | all-to-all | bytes 4194304 | tf_op jit(solution)/shard_map/all_to_all | solution.py:53
  85.5 1.4 shard_map.76
  86.9 0.1 broadcast_in_dim.33
  87.0 13.5 %all_to_all.32.hidden = bf16[4,256,512]{2,1,0:T(8,128)(2,1)S(1)} all-to-all(bf16[4,256,512]{2,1,0:T(8,128)(2,1)S(1)} %broadcast_in_dim.33), channel_id=1, replica_groups={{0,1,4,5},{2,3,6,7},{8,9,12,13},{10,11,14,15},{16,17,20,21},{18,19,22,2..., dimensions={0} | all-to-all | bytes 2097152 | tf_op jit(solution)/shard_map/all_to_all | solution.py:53
  100.5 0.0 copy-start.5
  100.5 1.5 shard_map.77
  102.0 8.4 %all-to-all-start.4 = ((bf16[8,64,512]{2,1,0:T(8,128)(2,1)}), bf16[8,64,512]{2,1,0:T(8,128)(2,1)S(1)}, u32[]{:S(2)}, u32[]{:S(2)}) async-start(bf16[8,64,512]{2,1,0:T(8,128)(2,1)} %bitcast.13), calls=%async_computation.4 | async-start | bytes 1048576 | tf_op jit(solution)/shard_map/all_to_all | solution.py:228
  110.4 0.0 copy-done.5
  110.4 13.9 %all-to-all-done.4 = bf16[8,64,512]{2,1,0:T(8,128)(2,1)S(1)} async-done(((bf16[8,64,512]{2,1,0:T(8,128)(2,1)}), bf16[8,64,512]{2,1,0:T(8,128)(2,1)S(1)}, u32[]{:S(2)}, u32[]{:S(2)}) %all-to-all-start.4) | async-done | bytes 524320 | tf_op jit(solution)/shard_map/all_to_all | solution.py:228
  124.3 0.1 convert_reduce_fusion
  124.4 2.8 %collective-permute-start.5 = (bf16[64,512]{1,0:T(8,128)(2,1)S(1)}, bf16[64,512]{1,0:T(8,128)(2,1)S(1)}, u32[]{:S(2)}, u32[]{:S(2)}) collective-permute-start(bf16[64,512]{1,0:T(8,128)(2,1)S(1)} %multiply_convert_fusion.mine), channel_id=1, source_target_pairs={{0,32},{32,0},{1,33},{33,1},{2,34},{34,2},{3,35},{35,3},{4,36},{36... | collective-permute-start | bytes 196616 | tf_op jit(solution)/shard_map/ppermute | solution.py:233
  127.3 0.9 collective-permute-done.5.other
  128.1 1.5 shard_map.78
  129.6 25.0 %all_to_all.33 = bf16[12,64,168]{2,1,0:T(8,128)(2,1)S(1)} all-to-all(bf16[12,64,168]{2,1,0:T(8,128)(2,1)S(1)} %shard_map.78), channel_id=1, replica_groups=mesh['z'=12,'core'=2,'y'=8,'x'=4] {'z'}, dimensions={0} | all-to-all | bytes 516096 | tf_op jit(solution)/shard_map/all_to_all | solution.py:241
  154.7 0.7 reduce_sum.22
  (5 shorter events, 0.1 us)
Async XLA Ops:
  1.5 38.4 %all-to-all-start = ((bf16[12,64,168]{2,1,0:T(8,128)(2,1)}), bf16[12,64,168]{2,1,0:T(8,128)(2,1)S(1)}, u32[]{:S(2)}, u32[]{:S(2)}) async-start(bf16[12,64,168]{2,1,0:T(8,128)(2,1)} %broadcast_in_dim.12), calls=%async_computation | async-start | bytes 786432 | tf_op jit(solution)/shard_map/all_to_all | solution.py:53
  17.3 1.2 copy-start.3
  18.5 12.7 %copy-start.4 = (s32[1,504]{1,0:T(1,128)S(1)}, s32[1,504]{1,0:T(1,128)}, u32[]{:S(2)}) copy-start(s32[1,504]{1,0:T(1,128)} %param.9) | copy-start | bytes 6052
  18.5 14.7 %copy-start = (bf16[1,2048,256]{2,1,0:T(8,128)(2,1)S(1)}, bf16[1,2048,256]{2,1,0:T(8,128)(2,1)}, u32[]{:S(2)}) copy-start(bf16[1,2048,256]{2,1,0:T(8,128)(2,1)} %param.11) | copy-start | bytes 3145732
  18.5 14.7 %copy-start.1 = (bf16[1,2048,256]{2,1,0:T(8,128)(2,1)S(1)}, bf16[1,2048,256]{2,1,0:T(8,128)(2,1)}, u32[]{:S(2)}) copy-start(bf16[1,2048,256]{2,1,0:T(8,128)(2,1)} %param.12) | copy-start | bytes 3145732
  19.8 14.8 %collective-permute-start = (bf16[512,256]{1,0:T(8,128)(2,1)}, bf16[512,256]{1,0:T(8,128)(2,1)S(1)}, u32[]{:S(2)}, u32[]{:S(2)}) collective-permute-start(bf16[512,256]{1,0:T(8,128)(2,1)} %get-tuple-element.23), channel_id=1, source_target_pairs={{0,1},{1,0},{4,5},{5,4},{2,3},{3,2},{6,7},{7,6},{8,9},{9,8},{12,13... | collective-permute-start | bytes 786440 | tf_op jit(solution)/shard_map/ppermute | solution.py:191
  24.2 10.4 %collective-permute-start.1 = (bf16[512,256]{1,0:T(8,128)(2,1)}, bf16[512,256]{1,0:T(8,128)(2,1)S(1)}, u32[]{:S(2)}, u32[]{:S(2)}) collective-permute-start(bf16[512,256]{1,0:T(8,128)(2,1)} %get-tuple-element.22), channel_id=1, source_target_pairs={{0,4},{1,5},{4,0},{5,1},{2,6},{3,7},{6,2},{7,3},{8,12},{9,13},{12,... | collective-permute-start | bytes 786440 | tf_op jit(solution)/shard_map/ppermute | solution.py:191
  29.3 10.6 %collective-permute-start.2 = (bf16[512,256]{1,0:T(8,128)(2,1)}, bf16[512,256]{1,0:T(8,128)(2,1)S(1)}, u32[]{:S(2)}, u32[]{:S(2)}) collective-permute-start(bf16[512,256]{1,0:T(8,128)(2,1)} %get-tuple-element.21), channel_id=1, source_target_pairs={{0,5},{1,4},{4,1},{5,0},{2,7},{3,6},{6,3},{7,2},{8,13},{9,12},{12,... | collective-permute-start | bytes 786440 | tf_op jit(solution)/shard_map/ppermute | solution.py:191
  31.2 8.7 %collective-permute-start.3 = (s32[1,512]{1,0:T(1,128)S(1)}, s32[1,512]{1,0:T(1,128)S(1)}, u32[]{:S(2)}, u32[]{:S(2)}) collective-permute-start(s32[1,512]{1,0:T(1,128)S(1)} %pad.8.own_ref), channel_id=1, source_target_pairs={{0,32},{32,0},{1,33},{33,1},{2,34},{34,2},{3,35},{35,3},{4,36},{36... | collective-permute-start | bytes 6152 | tf_op jit(solution)/shard_map/ppermute | solution.py:178
  33.2 0.7 copy-start.6
  39.9 0.8 copy-start.2
  41.7 3.1 %collective-permute-start.4 = (bf16[64,512]{1,0:T(8,128)(2,1)S(1)}, bf16[64,512]{1,0:T(8,128)(2,1)S(1)}, u32[]{:S(2)}, u32[]{:S(2)}) collective-permute-start(bf16[64,512]{1,0:T(8,128)(2,1)S(1)} %get-tuple-element.15), channel_id=1, source_target_pairs={{0,32},{32,0},{1,33},{33,1},{2,34},{34,2},{3,35},{35,3},{4,36},{36... | collective-permute-start | bytes 196616 | tf_op jit(solution)/shard_map/ppermute | solution.py:209
  100.5 9.9 %copy-start.5 = (f32[1,504]{1,0:T(1,128)S(1)}, f32[1,504]{1,0:T(1,128)}, u32[]{:S(2)}) copy-start(f32[1,504]{1,0:T(1,128)} %param.10) | copy-start | bytes 6052
  102.0 22.3 %all-to-all-start.4 = ((bf16[8,64,512]{2,1,0:T(8,128)(2,1)}), bf16[8,64,512]{2,1,0:T(8,128)(2,1)S(1)}, u32[]{:S(2)}, u32[]{:S(2)}) async-start(bf16[8,64,512]{2,1,0:T(8,128)(2,1)} %bitcast.13), calls=%async_computation.4 | async-start | bytes 1048576 | tf_op jit(solution)/shard_map/all_to_all | solution.py:228
  124.4 3.7 %collective-permute-start.5 = (bf16[64,512]{1,0:T(8,128)(2,1)S(1)}, bf16[64,512]{1,0:T(8,128)(2,1)S(1)}, u32[]{:S(2)}, u32[]{:S(2)}) collective-permute-start(bf16[64,512]{1,0:T(8,128)(2,1)S(1)} %multiply_convert_fusion.mine), channel_id=1, source_target_pairs={{0,32},{32,0},{1,33},{33,1},{2,34},{34,2},{3,35},{35,3},{4,36},{36... | collective-permute-start | bytes 196616 | tf_op jit(solution)/shard_map/ppermute | solution.py:233

commit v2 on v1

v2 whole, which is shorter than its diff:
```python
import functools

import jax
import jax.numpy as jnp
from jax import lax
from jax.experimental import pallas as pl
from jax.experimental.pallas import tpu as pltpu
from jax.sharding import Mesh, PartitionSpec as P


EPS = 1e-06
SLOTS = 512
HALF = 88
SIDE = 24
VMEM = pl.BlockSpec(memory_space=pltpu.VMEM)
SMEM = pl.BlockSpec(memory_space=pltpu.SMEM)
BF16 = jnp.bfloat16
F32 = jnp.float32
PLANE = ("core", "y", "x")


def call(kernel, outs, args, specs=None, scratch=(), flops=0, vmem=16):
    return pl.pallas_call(
        kernel,
        out_shape=outs,
        in_specs=specs or [VMEM] * len(args),
        out_specs=jax.tree.map(lambda _: VMEM, outs),
        scratch_shapes=list(scratch),
        compiler_params=pltpu.CompilerParams(vmem_limit_bytes=vmem * 1024 * 1024),
        cost_estimate=pl.CostEstimate(flops=flops, bytes_accessed=0, transcendentals=0),
    )(*args)


def place(core, y, x, ny, nx):
    return ((y + core) % ny) * nx + (x + core) % nx


def tiles(ny, nx):
    near, far = [], []
    for c in range(2):
        base = c * ny * nx

        def at(Y, X, b, a, c=c, base=base):
            return base + place(c, 2 * Y + b, 2 * X + a, ny, nx)

        corners = [(b, a) for b in range(2) for a in range(2)]
        cells = [(Y, X) for Y in range(ny // 2) for X in range(nx // 2)]
        near += [[at(Y, X, b, a) for b, a in corners] for Y, X in cells]
        far += [[at(Y, X, b, a) for Y, X in cells] for b, a in corners]
    return near, far


def hot(ids, base, rows):
    row = lax.broadcasted_iota(jnp.int32, (rows, ids.shape[1]), 0)
    return jnp.where(row == ids - base, 1.0, 0.0).astype(BF16)


def pack_kernel(tokens, chosen, out, ids):
    copies, part = out.shape[0], tokens.shape[0]
    ids[...] = jnp.full(ids.shape, 4095, jnp.int32)
    ids[:, : chosen.shape[1]] = chosen[...]
    turned = tokens[...].astype(F32).T
    rest = turned.shape[0] - HALF
    upper = jnp.concatenate([turned[HALF:], jnp.zeros((HALF - rest, part), F32)], axis=0)
    rows = jnp.concatenate([turned[:HALF], upper], axis=1)
    high = (ids[...] >> 6).astype(F32)
    low = (ids[...] & 63).astype(F32)
    lists = [v[:, k : k + 128] for v in (high, low) for k in range(0, SLOTS, 128)]
    body = jnp.concatenate([rows, *lists], axis=0).astype(BF16)
    for k in range(copies):
        out[k] = body


def send_hot_kernel(tok_dev, ids, low, high):
    side = ids.shape[1]
    token = ids[...].astype(F32)
    owner = jnp.floor((token + 0.5) * (1.0 / tok_dev))
    column = jnp.broadcast_to(token, (128, side)).T[:, :1]
    column_owner = jnp.broadcast_to(owner, (128, side)).T[:, :1]
    before = (column < token) & (column_owner == owner)
    rank = jnp.sum(jnp.where(before, 1.0, 0.0), axis=0, keepdims=True)
    code = (owner * (2.0 * SIDE) + rank).astype(jnp.int32)
    row = lax.broadcasted_iota(jnp.int32, (SIDE, side), 0)
    for o in range(low.shape[0]):
        low[o] = jnp.where(code == row + 2 * SIDE * o, 1.0, 0.0).astype(BF16)
        high[o] = jnp.where(code == row + 2 * SIDE * o + SIDE, 1.0, 0.0).astype(BF16)


def pick(tok_dev, core, gathered, ids, part):
    dims = (((0,), (0,)), ((), ()))
    acc = jnp.zeros((part, SLOTS), F32)
    for b in range(gathered.shape[0]):
        for half in range(2):
            base = (2 * b + core) * tok_dev + half * HALF
            rows = gathered[b, :HALF, half * part : (half + 1) * part]
            acc += lax.dot_general(rows, hot(ids, base, HALF), dims, preferred_element_type=F32)
    return acc


def pick_kernel(tok_dev, core_ref, gathered, ids, gain, mine):
    part = gain.shape[1]
    acc = pick(tok_dev, core_ref[0], gathered, ids[...], part)
    square = (part, part)
    same = lax.broadcasted_iota(jnp.int32, square, 0) == lax.broadcasted_iota(jnp.int32, square, 1)
    column = jnp.sum(jnp.where(same, gain[...], 0.0), axis=1, keepdims=True)
    high = column.astype(BF16)
    rest = column - high.astype(F32)
    middle = rest.astype(BF16)
    low = (rest - middle.astype(F32)).astype(BF16)
    lane = lax.broadcasted_iota(jnp.int32, mine.shape, 1)
    first = SLOTS - 8
    acc = jnp.where(lane == first, high.astype(F32), acc)
    acc = jnp.where(lane == first + 1, middle.astype(F32), acc)
    mine[...] = jnp.where(lane == first + 2, low.astype(F32), acc)


def pick_other_kernel(tok_dev, core_ref, swapped, ids, mine, out):
    acc = pick(tok_dev, 1 - core_ref[0], swapped, ids[...], mine.shape[0])
    total = (acc + mine[...]).astype(BF16)
    for g in range(out.shape[0]):
        out[g] = total


def member_kernel(plane_ref, core_ref, gathered, swapped, low, high):
    blocks = gathered.shape[0]
    tokens = low.shape[0]
    core = core_ref[0]
    base = (2 * plane_ref[0] + core) * tokens
    token = (lax.broadcasted_iota(jnp.int32, (tokens, 128), 0) + base).astype(F32)
    expert = lax.broadcasted_iota(jnp.int32, (tokens, 128), 1)
    member = jnp.zeros((tokens, 128), F32)
    for source in range(2):
        for b in range(blocks):
            lists = (gathered, swapped)[source][b, HALF : HALF + 8, :].astype(F32)
            ids = lists[:4] * 64.0 + lists[4:]
            found = jnp.zeros((tokens, 128), F32)
            for k in range(4):
                found += jnp.where(token == ids[k : k + 1], 1.0, 0.0)
            count = jnp.sum(found, axis=1, keepdims=True)
            which = 2 * b + (core if source == 0 else 1 - core)
            member += jnp.where(expert == which, count, 0.0)
    triangle = (tokens, tokens)
    earlier = lax.broadcasted_iota(jnp.int32, triangle, 1) < lax.broadcasted_iota(
        jnp.int32, triangle, 0
    )
    rank = jnp.dot(
        jnp.where(earlier, 1.0, 0.0).astype(BF16), member.astype(BF16), preferred_element_type=F32
    )
    slot = jnp.where(member > 0.5, rank, 255.0).astype(BF16)
    spread = (128, low.shape[1])
    line = lax.broadcasted_iota(jnp.int32, spread, 0) * SIDE
    place = lax.broadcasted_iota(jnp.int32, spread, 1)
    inside = (place >= line) & (place < line + SIDE)
    slots = jnp.dot(slot, jnp.where(inside, 1.0, 0.0).astype(BF16), preferred_element_type=F32)
    start = jnp.zeros(spread, jnp.int32) + jnp.where(inside, place - line, 0)
    start = jnp.sum(start.astype(F32), axis=0, keepdims=True)
    low[...] = jnp.where(slots == start, 1.0, 0.0).astype(BF16)
    high[...] = jnp.where(slots == start + float(SIDE), 1.0, 0.0).astype(BF16)


def block_of(core, corner, cell, ny, nx):
    Y, X = cell // (nx // 2), cell % (nx // 2)
    b, a = corner // 2, corner % 2
    return place(core, 2 * Y + b, 2 * X + a, ny, nx)


def turn_kernel(ny, nx, core_ref, gate_ref, up_ref, out):
    _, _, hid = gate_ref.shape
    cells = ny * nx // 4
    for s in range(4):
        for half, ref in enumerate((gate_ref, up_ref)):
            pieces = [ref[block_of(core_ref[0], s, g, ny, nx)] for g in range(cells)]
            rows = jnp.concatenate(pieces, axis=0)
            out[s, half * hid : (half + 1) * hid] = rows.T


def turn_down_kernel(ny, nx, core_ref, corner_ref, down_ref, w0, w1, w2, w3, turned):
    tp, part, hid = turned.shape
    for y in range(ny):
        rows = down_ref[:, y * nx * part : (y + 1) * nx * part].T
        turned[y * nx : (y + 1) * nx] = rows.reshape(nx, part, hid)
    for flip, out in enumerate((w0, w1, w2, w3)):
        for g in range(tp // 4):
            block = block_of(core_ref[0], corner_ref[0] ^ flip, g, ny, nx)
            out[g * part : (g + 1) * part] = turned[block]


def copies_kernel(array, out):
    for k in range(out.shape[0]):
        out[k] = array[...]


def hidden_kernel(x_ref, w_ref, out, normed):
    corners, depth, slots = x_ref.shape
    hid = out.shape[1]
    width = corners * depth
    square = jnp.zeros((1, slots), F32)
    for s in range(corners):
        v = x_ref[s].astype(F32)
        square += jnp.sum(v * v, axis=0, keepdims=True)
    scale = lax.rsqrt(square / width + EPS)
    acc = jnp.zeros((2 * hid, slots), F32)
    for s in range(corners):
        v = x_ref[s]
        parts = v[:, slots - 128 :].astype(F32)
        lane = lax.broadcasted_iota(jnp.int32, parts.shape, 1)
        keep = (lane >= 120) & (lane < 123)
        gain = jnp.sum(jnp.where(keep, parts, 0.0), axis=1, keepdims=True)
        normed[...] = (v.astype(F32) * scale * gain).astype(BF16)
        acc += jnp.dot(w_ref[s], normed[...], preferred_element_type=F32)
    gate, up = acc[:hid], acc[hid:]
    value = (gate / (1.0 + jnp.exp(-gate)) * up).astype(BF16)
    for k in range(out.shape[0]):
        out[k] = value


def down_kernel(corner_ref, hidden, w0, w1, w2, w3, out):
    me = corner_ref[0]
    acc = jnp.zeros(out.shape, F32)
    for flip, w in enumerate((w0, w1, w2, w3)):
        acc += jnp.dot(w[...], hidden[me ^ flip], preferred_element_type=F32)
    out[...] = acc.astype(BF16)


def send_kernel(arrived, affinity, low, high, out, weight):
    weight[...] = jnp.zeros(weight.shape, F32)
    weight[:, : affinity.shape[1]] = affinity[...]
    total = arrived[0].astype(F32)
    for g in range(1, arrived.shape[0]):
        total += arrived[g].astype(F32)
    weighted = (total * weight[...]).astype(BF16)
    empty = jnp.zeros_like(weighted)
    dims = (((1,), (1,)), ((), ()))
    rows = lax.dot_general(
        low[...],
        jnp.concatenate([weighted, empty], axis=0),
        dims,
        preferred_element_type=F32,
    )
    rows += lax.dot_general(
        high[...],
        jnp.concatenate([empty, weighted], axis=0),
        dims,
        preferred_element_type=F32,
    )
    out[...] = rows.astype(BF16)


def final_kernel(arrived, low, high, out):
    part = out.shape[0]
    total = jnp.dot(low[...], arrived[...], preferred_element_type=F32)[:, :part]
    total += jnp.dot(high[...], arrived[...], preferred_element_type=F32)[:, part:]
    out[...] = total.T.astype(BF16)


def local(tokens, norm_gain, chosen, affinity, w_gate, w_up, w_down):
    tok_dev, part = tokens.shape
    nz, ny, nx = lax.axis_size("z"), lax.axis_size("y"), lax.axis_size("x")
    experts = 2 * nz
    width, hid = w_gate.shape[1:]
    tp, cells = ny * nx, ny * nx // 4
    near, far = tiles(ny, nx)
    swap = [(0, 1), (1, 0)]
    core_index = lax.axis_index("core").astype(jnp.int32)
    z_index = lax.axis_index("z").astype(jnp.int32)
    y_index = lax.axis_index("y").astype(jnp.int32)
    x_index = lax.axis_index("x").astype(jnp.int32)
    corner_index = ((y_index + core_index) & 1) * 2 + ((x_index + core_index) & 1)
    core, corner = core_index.reshape(1), corner_index.reshape(1)
    plane = z_index.reshape(1)

    packed, own_ids = call(
        pack_kernel,
        [
            jax.ShapeDtypeStruct((nz, HALF + 8, 128), BF16),
            jax.ShapeDtypeStruct((1, SLOTS), jnp.int32),
        ],
        (tokens.T, chosen),
    )
    gathered = lax.all_to_all(packed, "z", 0, 0, tiled=True)

    down_shape = jax.ShapeDtypeStruct((cells * part, hid), BF16)
    downs = list(call(
        functools.partial(turn_down_kernel, ny, nx),
        [down_shape] * 4,
        (core, corner, w_down[0]),
        [SMEM, SMEM, VMEM],
        [pltpu.VMEM((tp, part, hid), BF16)],
        flops=1 << 30,
    ))
    for flip in range(1, 4):
        pairs = [(g[s], g[s ^ flip]) for g in near for s in range(4)]
        downs[flip] = lax.ppermute(downs[flip], PLANE, pairs)
    turned = call(
        functools.partial(turn_kernel, ny, nx),
        jax.ShapeDtypeStruct((4, 2 * hid, cells * part), BF16),
        (core, w_gate[0].reshape(tp, part, hid), w_up[0].reshape(tp, part, hid)),
        [SMEM, VMEM, VMEM],
        flops=1 << 30,
    )
    gathered, turned = lax.optimization_barrier((gathered, turned))

    swapped = lax.ppermute(gathered, "core", swap)
    own = call(
        functools.partial(pick_kernel, tok_dev),
        jax.ShapeDtypeStruct((part, SLOTS), F32),
        (core, gathered, own_ids, norm_gain[None]),
        [SMEM] + [VMEM] * 3,
        flops=2 * part * nz * tok_dev * SLOTS,
    )
    picked = call(
        functools.partial(pick_other_kernel, tok_dev),
        jax.ShapeDtypeStruct((cells, part, SLOTS), BF16),
        (core, swapped, own_ids, own),
        [SMEM] + [VMEM] * 3,
        flops=2 * part * nz * tok_dev * SLOTS,
    )

    column = lax.all_to_all(
        picked, PLANE, 0, 0, axis_index_groups=far, tiled=True
    ).reshape(cells * part, SLOTS)
    column, downs = lax.optimization_barrier((column, downs))
    copies = call(
        copies_kernel,
        jax.ShapeDtypeStruct((4, cells * part, SLOTS), BF16),
        (column,),
        flops=1 << 20,
    )
    full = lax.all_to_all(copies, PLANE, 0, 0, axis_index_groups=near, tiled=True)
    hidden = call(
        hidden_kernel,
        jax.ShapeDtypeStruct((4, hid, SLOTS), BF16),
        (full, turned),
        scratch=[pltpu.VMEM((cells * part, SLOTS), BF16)],
        flops=4 * width * hid * SLOTS,
    )
    tile_hidden = lax.all_to_all(hidden, PLANE, 0, 0, axis_index_groups=near, tiled=True)
    partial = call(
        down_kernel,
        jax.ShapeDtypeStruct((cells * part, SLOTS), BF16),
        (corner, tile_hidden, *downs),
        [SMEM] + [VMEM] * 5,
        flops=2 * width * hid * SLOTS,
    )
    late = lax.optimization_barrier((partial, own_ids, gathered, swapped))
    partial, own_ids, gathered, swapped = late
    arrived = lax.all_to_all(
        partial.reshape(cells, part, SLOTS), PLANE, 0, 0, axis_index_groups=far, tiled=True
    )
    hot_shape = jax.ShapeDtypeStruct((experts, SIDE, SLOTS), BF16)
    send_hot = call(
        functools.partial(send_hot_kernel, tok_dev),
        [hot_shape, hot_shape],
        (own_ids,),
        flops=1 << 30,
    )
    send_hot = [v.reshape(experts * SIDE, SLOTS) for v in send_hot]
    hot_shape = jax.ShapeDtypeStruct((tok_dev, experts * SIDE), BF16)
    final_hot = call(
        member_kernel,
        [hot_shape, hot_shape],
        (plane, core, gathered, swapped),
        [SMEM, SMEM, VMEM, VMEM],
        flops=1 << 31,
    )
    sent = call(
        send_kernel,
        jax.ShapeDtypeStruct((experts * SIDE, 128), BF16),
        (arrived, affinity, *send_hot),
        scratch=[pltpu.VMEM((1, SLOTS), F32)],
        flops=4 * 128 * experts * SIDE * SLOTS,
    )
    back = lax.all_to_all(
        sent.reshape(experts, SIDE, 128), ("z", "core"), 0, 0, tiled=True
    ).reshape(experts * SIDE, 128)
    total = call(
        final_kernel,
        jax.ShapeDtypeStruct((part, tok_dev), BF16),
        (back, *final_hot),
        flops=4 * 128 * experts * SIDE * tok_dev,
    )
    return total.T


def solution(mesh):
    nz, ny, nx = 12, 8, 4
    fine = Mesh(mesh.devices.reshape(nz, 2, ny, nx), ("z", "core", "y", "x"))
    ep, tp = ("z", "core"), ("y", "x")
    in_specs = (
        P(ep, tp),
        P(tp),
        P(ep, None),
        P(ep, None),
        P(ep, None, tp),
        P(ep, None, tp),
        P(ep, tp, None),
    )

    return jax.shard_map(local, mesh=fine, in_specs=in_specs, out_specs=P(ep, tp), check_vma=False)
```

time: 158 us -> 150 us (0.949)
  blocking collectives: 78.9 us -> 32.3 us
  waiting for transfers between devices: 21.4 us -> 45.9 us
  starting transfers between devices: 42.1 us -> 51.4 us
  Pallas kernels: 6.4 us -> 11.8 us
  local copies, waits for them, and re-layouts: 5.48 us -> 7.25 us
    all_to_all x4 -> x2, blocking collectives: 78.9 us -> 32.3 us  [the longest x1 18.5 us: local(): lax.all_to_all(copies, PLANE, 0, 0, axis_index_groups=near, tiled=True)]
    all_to_all x1 -> x3, waiting for transfers between devices: 0.01 us -> 23.8 us  [the longest x1 12.6 us: local(): gathered = lax.all_to_all(packed, 'z', 0, 0, tiled=True)]
    all_to_all x1 -> x3, starting transfers between devices: 15.7 us -> 29.6 us  [the longest x1 15.7 us: local(): gathered = lax.all_to_all(packed, 'z', 0, 0, tiled=True)]
    pallas_call x6 -> x12, Pallas kernels: 6.4 us -> 11.8 us  [call(): pl.pallas_call(kernel, out_shape=outs, in_specs=specs or [VMEM] * len(arg...]
    unnamed x14 -> x26, local copies, waits for them, and re-layouts: 2.04 us -> 7.25 us
    ppermute x6 -> x4, starting transfers between devices: 18.1 us -> 14.9 us  [the longest x3 10.8 us: local(): downs[flip] = lax.ppermute(downs[flip], PLANE, pairs)]
    broadcast_in_dim x5 -> x0, local copies, waits for them, and re-layouts: 2.51 us -> none  [the longest x4 1.81 us: to_all(): jnp.broadcast_to(array[None], (n, *array.shape))]
    ppermute x6 -> x4, waiting for transfers between devices: 7.48 us -> 8.87 us  [the longest x3 8.58 us: local(): downs[flip] = lax.ppermute(downs[flip], PLANE, pairs)]
  transfers between devices with their start and end apart: 8 -> 8, of which waited for: 4 -> 6; matrix products, arithmetic and copies ran while one was open for 1% -> 0% of each run, Pallas kernels for 1% -> 3%
where the time goes in v2:
time: 150 us; the launch traced here: 149 us
  starting transfers between devices  51.4 us (34%)
  waiting for transfers between devices  45.9 us (31%)
  blocking collectives  32.3 us (22%)
  Pallas kernels  11.8 us (8%)
  local copies, waits for them, and re-layouts  7.25 us (5%)
    all_to_all x1, blocking collectives, local(): lax.all_to_all(copies, PLANE, 0, 0, axis_index_groups=near, tiled=True)  18.5 us
    all_to_all x1, starting transfers between devices, local(): gathered = lax.all_to_all(packed, 'z', 0, 0, tiled=True)  15.7 us
    all_to_all x1, blocking collectives, local(): lax.all_to_all(hidden, PLANE, 0, 0, axis_index_groups=near, tiled=True)  13.8 us
    all_to_all x1, waiting for transfers between devices, local(): lax.all_to_all(partial.reshape(cells, part, SLOTS), PLANE, 0, 0, axis_ind...  13.2 us
    all_to_all x1, waiting for transfers between devices, local(): gathered = lax.all_to_all(packed, 'z', 0, 0, tiled=True)  12.6 us
    pallas_call x12, Pallas kernels, call(): pl.pallas_call(kernel, out_shape=outs, in_specs=specs or [VMEM] * len(arg...  11.8 us
    all_to_all x1, waiting for transfers between devices, local(): lax.all_to_all(sent.reshape(experts, SIDE, 128), ('z', 'core'), 0, 0, til...  11.2 us
    ppermute x3, starting transfers between devices, local(): downs[flip] = lax.ppermute(downs[flip], PLANE, pairs)  10.8 us
  transfers between devices with their start and end apart: 8, of which 6 were waited for; matrix products, arithmetic and copies ran while one was open for 0% of the time, Pallas kernels for 3%

profile of v2, /device:TPU:1, one launch (start us, length us, event | category | flops | bytes accessed | tf_op | source)
XLA Modules:
  0.0 148.8 jit_solution(4850112685783582088)
XLA Ops:
  0.0 0.8 copy-done.8
  0.8 0.7 copy-done.9
  1.4 0.9 shard_map.73
  2.3 15.7 %all-to-all-start = ((bf16[12,96,128]{2,1,0:T(8,128)(2,1)}), bf16[12,96,128]{2,1,0:T(8,128)(2,1)S(1)}, u32[]{:S(2)}, u32[]{:S(2)}) async-start(bf16[12,96,128]{2,1,0:T(8,128)(2,1)} %get-tuple-element.26), calls=%async_computation | async-start | bytes 589824 | tf_op jit(solution)/shard_map/all_to_all | solution.py:280
  18.1 0.0 copy-start
  18.1 1.2 copy-done
  19.3 1.2 copy-done.1
  20.5 0.6 shard_map.74.w_ref
  21.1 12.6 %all-to-all-done.gathered = bf16[12,96,128]{2,1,0:T(8,128)(2,1)S(1)} async-done(((bf16[12,96,128]{2,1,0:T(8,128)(2,1)}), bf16[12,96,128]{2,1,0:T(8,128)(2,1)S(1)}, u32[]{:S(2)}, u32[]{:S(2)}) %all-to-all-start) | async-done | bytes 294944 | tf_op jit(solution)/shard_map/all_to_all | solution.py:280
  33.7 4.1 %collective-permute-start = (bf16[12,96,128]{2,1,0:T(8,128)(2,1)S(1)}, bf16[12,96,128]{2,1,0:T(8,128)(2,1)S(1)}, u32[]{:S(2)}, u32[]{:S(2)}) collective-permute-start(bf16[12,96,128]{2,1,0:T(8,128)(2,1)S(1)} %all-to-all-done.gathered), channel_id=1, source_target_pairs={{0,32},{32,0},{1,33},{33,1},{2,34},{34,2},{3,35},{35,3},{4,36},{36... | collective-permute-start | bytes 884744 | tf_op jit(solution)/shard_map/ppermute | solution.py:303
  37.8 0.0 copy-done.12
  37.9 0.9 shard_map.75.mine
  38.7 0.3 collective-permute-done.swapped
  39.0 1.7 %shard_map.76 = bf16[8,64,512]{2,1,0:T(8,128)(2,1)} custom-call(s32[1]{0:T(128)} %bitcast.1.core_ref, bf16[12,96,128]{2,1,0:T(8,128)(2,1)S(1)} %collective-permute-done.swapped, s32[1,512]{1,0:T(1,128)S(1)} %get-tuple-element.40.ids, f32[64,512]{1,0:T(8,128)S(1)} %shard_map.75.mine), custom_call_target="tpu_custom_call" | custom-call | flops 132120576 | tf_op jit(solution)/shard_map/pallas_call | solution.py:23
  40.7 9.8 %all-to-all-start.1 = ((bf16[8,64,512]{2,1,0:T(8,128)(2,1)}), bf16[8,64,512]{2,1,0:T(8,128)(2,1)S(1)}, u32[]{:S(2)}, u32[]{:S(2)}) async-start(bf16[8,64,512]{2,1,0:T(8,128)(2,1)} %shard_map.76), calls=%async_computation.1 | async-start | bytes 1048576 | tf_op jit(solution)/shard_map/all_to_all | solution.py:319
  50.5 1.2 copy-done.11
  51.8 0.4 shard_map.77
  52.2 4.3 %collective-permute-start.1 = (bf16[512,256]{1,0:T(8,128)(2,1)S(1)}, bf16[512,256]{1,0:T(8,128)(2,1)S(1)}, u32[]{:S(2)}, u32[]{:S(2)}) collective-permute-start(bf16[512,256]{1,0:T(8,128)(2,1)S(1)} %get-tuple-element.30), channel_id=1, source_target_pairs={{0,1},{1,0},{4,5},{5,4},{2,3},{3,2},{6,7},{7,6},{8,9},{9,8},{12,13... | collective-permute-start | bytes 786440 | tf_op jit(solution)/shard_map/ppermute | solution.py:293
  56.5 4.2 %collective-permute-start.2 = (bf16[512,256]{1,0:T(8,128)(2,1)S(1)}, bf16[512,256]{1,0:T(8,128)(2,1)S(1)}, u32[]{:S(2)}, u32[]{:S(2)}) collective-permute-start(bf16[512,256]{1,0:T(8,128)(2,1)S(1)} %get-tuple-element.31), channel_id=1, source_target_pairs={{0,4},{1,5},{4,0},{5,1},{2,6},{3,7},{6,2},{7,3},{8,12},{9,13},{12,... | collective-permute-start | bytes 786440 | tf_op jit(solution)/shard_map/ppermute | solution.py:293
  60.7 2.3 %collective-permute-start.3 = (bf16[512,256]{1,0:T(8,128)(2,1)S(1)}, bf16[512,256]{1,0:T(8,128)(2,1)S(1)}, u32[]{:S(2)}, u32[]{:S(2)}) collective-permute-start(bf16[512,256]{1,0:T(8,128)(2,1)S(1)} %get-tuple-element.32), channel_id=1, source_target_pairs={{0,5},{1,4},{4,1},{5,0},{2,7},{3,6},{6,3},{7,2},{8,13},{9,12},{12,... | collective-permute-start | bytes 786440 | tf_op jit(solution)/shard_map/ppermute | solution.py:293
  63.0 0.0 collective-permute-done.1.w1
  63.0 0.0 copy-start.2
  63.0 0.7 copy-done.2
  63.7 5.3 %collective-permute-done.2.w2 = bf16[512,256]{1,0:T(8,128)(2,1)S(1)} collective-permute-done((bf16[512,256]{1,0:T(8,128)(2,1)S(1)}, bf16[512,256]{1,0:T(8,128)(2,1)S(1)}, u32[]{:S(2)}, u32[]{:S(2)}) %collective-permute-start.2) | collective-permute-done | bytes 262176 | tf_op jit(solution)/shard_map/ppermute | solution.py:293
  69.0 0.7 copy-done.4
  69.7 3.3 %collective-permute-done.3.w3 = bf16[512,256]{1,0:T(8,128)(2,1)S(1)} collective-permute-done((bf16[512,256]{1,0:T(8,128)(2,1)S(1)}, bf16[512,256]{1,0:T(8,128)(2,1)S(1)}, u32[]{:S(2)}, u32[]{:S(2)}) %collective-permute-start.3) | collective-permute-done | bytes 262176 | tf_op jit(solution)/shard_map/ppermute | solution.py:293
  73.0 0.7 copy-done.6
  73.7 0.0 all-to-all-done.1
  73.7 0.1 shard_map.78
  73.8 18.5 %all_to_all.30.x_ref = bf16[4,512,512]{2,1,0:T(8,128)(2,1)S(1)} all-to-all(bf16[4,512,512]{2,1,0:T(8,128)(2,1)S(1)} %shard_map.78), channel_id=1, replica_groups={{0,1,4,5},{2,3,6,7},{8,9,12,13},{10,11,14,15},{16,17,20,21},{18,19,22,2..., dimensions={0} | all-to-all | bytes 4194304 | tf_op jit(solution)/shard_map/all_to_all | solution.py:329
  92.4 1.4 shard_map.79
  93.8 0.0 copy-start.3
  93.8 0.0 copy-start.5
  93.8 0.0 copy-start.7
  93.8 13.8 %all_to_all.31.hidden = bf16[4,256,512]{2,1,0:T(8,128)(2,1)S(1)} all-to-all(bf16[4,256,512]{2,1,0:T(8,128)(2,1)S(1)} %shard_map.79), channel_id=1, replica_groups={{0,1,4,5},{2,3,6,7},{8,9,12,13},{10,11,14,15},{16,17,20,21},{18,19,22,2..., dimensions={0} | all-to-all | bytes 2097152 | tf_op jit(solution)/shard_map/all_to_all | solution.py:337
  107.6 0.0 copy-done.3
  107.6 0.0 copy-done.5
  107.6 0.0 copy-done.7
  107.6 1.5 %shard_map.80 = bf16[512,512]{1,0:T(8,128)(2,1)} custom-call(s32[1]{0:T(128)} %bitcast.corner_ref, bf16[4,256,512]{2,1,0:T(8,128)(2,1)S(1)} %all_to_all.31.hidden, bf16[512,256]{1,0:T(8,128)(2,1)S(1)} %get-tuple-element.35.w0, bf16[512,256]{1,0:T(8,128)(2,1)S(1)} %copy-done.3, bf16[512,256]{1,0:T(8,128)(2,1)S(1)} %copy-done.5, bf16[512,256]{1,0:T(8,128)(2,1)S(1)} %copy-done.7), custom_call_target="tpu_custom_call" | custom-call | flops 536870912 | tf_op jit(solution)/shard_map/pallas_call | solution.py:23
  109.1 6.9 %all-to-all-start.4 = ((bf16[8,64,512]{2,1,0:T(8,128)(2,1)}), bf16[8,64,512]{2,1,0:T(8,128)(2,1)S(1)}, u32[]{:S(2)}, u32[]{:S(2)}) async-start(bf16[8,64,512]{2,1,0:T(8,128)(2,1)} %bitcast.8), calls=%async_computation.4 | async-start | bytes 1048576 | tf_op jit(solution)/shard_map/all_to_all | solution.py:347
  116.0 0.7 shard_map.81
  116.8 13.2 %all-to-all-done.4.arrived = bf16[8,64,512]{2,1,0:T(8,128)(2,1)S(1)} async-done(((bf16[8,64,512]{2,1,0:T(8,128)(2,1)}), bf16[8,64,512]{2,1,0:T(8,128)(2,1)S(1)}, u32[]{:S(2)}, u32[]{:S(2)}) %all-to-all-start.4) | async-done | bytes 524320 | tf_op jit(solution)/shard_map/all_to_all | solution.py:347
  129.9 0.0 copy-done.10
  129.9 1.1 shard_map.82
  131.1 4.1 %all-to-all-start.5 = ((bf16[24,24,128]{2,1,0:T(8,128)(2,1)}), bf16[24,24,128]{2,1,0:T(8,128)(2,1)S(1)}, u32[]{:S(2)}, u32[]{:S(2)}) async-start(bf16[24,24,128]{2,1,0:T(8,128)(2,1)} %bitcast.11), calls=%async_computation.5 | async-start | bytes 294912 | tf_op jit(solution)/shard_map/all_to_all | solution.py:373
  135.2 1.3 shard_map.83
  136.6 11.2 %all-to-all-done.5 = bf16[24,24,128]{2,1,0:T(8,128)(2,1)S(1)} async-done(((bf16[24,24,128]{2,1,0:T(8,128)(2,1)}), bf16[24,24,128]{2,1,0:T(8,128)(2,1)S(1)}, u32[]{:S(2)}, u32[]{:S(2)}) %all-to-all-start.5) | async-done | bytes 147488 | tf_op jit(solution)/shard_map/all_to_all | solution.py:373
  147.7 1.1 shard_map.84
  (8 shorter events, 0.0 us)
Async XLA Ops:
  0.0 0.8 copy-start.8
  0.8 0.7 copy-start.9
  2.3 31.4 %all-to-all-start = ((bf16[12,96,128]{2,1,0:T(8,128)(2,1)}), bf16[12,96,128]{2,1,0:T(8,128)(2,1)S(1)}, u32[]{:S(2)}, u32[]{:S(2)}) async-start(bf16[12,96,128]{2,1,0:T(8,128)(2,1)} %get-tuple-element.26), calls=%async_computation | async-start | bytes 589824 | tf_op jit(solution)/shard_map/all_to_all | solution.py:280
  18.1 1.2 copy-start
  19.3 1.2 copy-start.1
  20.5 17.3 %copy-start.12 = (f32[64]{0:T(128)S(1)}, f32[64]{0:T(128)}, u32[]{:S(2)}) copy-start(f32[64]{0:T(128)} %param.8) | copy-start | bytes 772
  33.7 5.3 %collective-permute-start = (bf16[12,96,128]{2,1,0:T(8,128)(2,1)S(1)}, bf16[12,96,128]{2,1,0:T(8,128)(2,1)S(1)}, u32[]{:S(2)}, u32[]{:S(2)}) collective-permute-start(bf16[12,96,128]{2,1,0:T(8,128)(2,1)S(1)} %all-to-all-done.gathered), channel_id=1, source_target_pairs={{0,32},{32,0},{1,33},{33,1},{2,34},{34,2},{3,35},{35,3},{4,36},{36... | collective-permute-start | bytes 884744 | tf_op jit(solution)/shard_map/ppermute | solution.py:303
  40.7 33.0 %all-to-all-start.1 = ((bf16[8,64,512]{2,1,0:T(8,128)(2,1)}), bf16[8,64,512]{2,1,0:T(8,128)(2,1)S(1)}, u32[]{:S(2)}, u32[]{:S(2)}) async-start(bf16[8,64,512]{2,1,0:T(8,128)(2,1)} %shard_map.76), calls=%async_computation.1 | async-start | bytes 1048576 | tf_op jit(solution)/shard_map/all_to_all | solution.py:319
  50.5 1.2 copy-start.11
  52.2 10.8 %collective-permute-start.1 = (bf16[512,256]{1,0:T(8,128)(2,1)S(1)}, bf16[512,256]{1,0:T(8,128)(2,1)S(1)}, u32[]{:S(2)}, u32[]{:S(2)}) collective-permute-start(bf16[512,256]{1,0:T(8,128)(2,1)S(1)} %get-tuple-element.30), channel_id=1, source_target_pairs={{0,1},{1,0},{4,5},{5,4},{2,3},{3,2},{6,7},{7,6},{8,9},{9,8},{12,13... | collective-permute-start | bytes 786440 | tf_op jit(solution)/shard_map/ppermute | solution.py:293
  56.5 12.5 %collective-permute-start.2 = (bf16[512,256]{1,0:T(8,128)(2,1)S(1)}, bf16[512,256]{1,0:T(8,128)(2,1)S(1)}, u32[]{:S(2)}, u32[]{:S(2)}) collective-permute-start(bf16[512,256]{1,0:T(8,128)(2,1)S(1)} %get-tuple-element.31), channel_id=1, source_target_pairs={{0,4},{1,5},{4,0},{5,1},{2,6},{3,7},{6,2},{7,3},{8,12},{9,13},{12,... | collective-permute-start | bytes 786440 | tf_op jit(solution)/shard_map/ppermute | solution.py:293
  60.7 12.3 %collective-permute-start.3 = (bf16[512,256]{1,0:T(8,128)(2,1)S(1)}, bf16[512,256]{1,0:T(8,128)(2,1)S(1)}, u32[]{:S(2)}, u32[]{:S(2)}) collective-permute-start(bf16[512,256]{1,0:T(8,128)(2,1)S(1)} %get-tuple-element.32), channel_id=1, source_target_pairs={{0,5},{1,4},{4,1},{5,0},{2,7},{3,6},{6,3},{7,2},{8,13},{9,12},{12,... | collective-permute-start | bytes 786440 | tf_op jit(solution)/shard_map/ppermute | solution.py:293
  63.0 0.7 copy-start.2
  69.0 0.7 copy-start.4
  73.0 0.7 copy-start.6
  93.8 13.8 %copy-start.3 = (bf16[512,256]{1,0:T(8,128)(2,1)S(1)}, bf16[512,256]{1,0:T(8,128)(2,1)}, u32[]{:S(2)}) copy-start(bf16[512,256]{1,0:T(8,128)(2,1)} %copy-done.2) | copy-start | bytes 786436
  93.8 13.8 %copy-start.5 = (bf16[512,256]{1,0:T(8,128)(2,1)S(1)}, bf16[512,256]{1,0:T(8,128)(2,1)}, u32[]{:S(2)}) copy-start(bf16[512,256]{1,0:T(8,128)(2,1)} %copy-done.4) | copy-start | bytes 786436
  93.8 13.8 %copy-start.7 = (bf16[512,256]{1,0:T(8,128)(2,1)S(1)}, bf16[512,256]{1,0:T(8,128)(2,1)}, u32[]{:S(2)}) copy-start(bf16[512,256]{1,0:T(8,128)(2,1)} %copy-done.6) | copy-start | bytes 786436
  109.1 20.8 %all-to-all-start.4 = ((bf16[8,64,512]{2,1,0:T(8,128)(2,1)}), bf16[8,64,512]{2,1,0:T(8,128)(2,1)S(1)}, u32[]{:S(2)}, u32[]{:S(2)}) async-start(bf16[8,64,512]{2,1,0:T(8,128)(2,1)} %bitcast.8), calls=%async_computation.4 | async-start | bytes 1048576 | tf_op jit(solution)/shard_map/all_to_all | solution.py:347
  116.0 13.9 %copy-start.10 = (f32[1,504]{1,0:T(1,128)S(1)}, f32[1,504]{1,0:T(1,128)}, u32[]{:S(2)}) copy-start(f32[1,504]{1,0:T(1,128)} %affinity.1) | copy-start | bytes 6052
  131.1 16.7 %all-to-all-start.5 = ((bf16[24,24,128]{2,1,0:T(8,128)(2,1)}), bf16[24,24,128]{2,1,0:T(8,128)(2,1)S(1)}, u32[]{:S(2)}, u32[]{:S(2)}) async-start(bf16[24,24,128]{2,1,0:T(8,128)(2,1)} %bitcast.11), calls=%async_computation.5 | async-start | bytes 294912 | tf_op jit(solution)/shard_map/all_to_all | solution.py:373

commit v3 on v2

--- a/solution.py
+++ b/solution.py
@@ -55,8 +55,16 @@
     return jnp.where(row == ids - base, 1.0, 0.0).astype(BF16)
 
 
-def pack_kernel(tokens, chosen, out, ids):
+def pack_kernel(tokens_ref, chosen_ref, out, ids, tokens, chosen, sems):
     copies, part = out.shape[0], tokens.shape[0]
+    loads = [
+        pltpu.make_async_copy(tokens_ref, tokens, sems.at[0]),
+        pltpu.make_async_copy(chosen_ref, chosen, sems.at[1]),
+    ]
+    for load in loads:
+        load.start()
+    for load in loads:
+        load.wait()
     ids[...] = jnp.full(ids.shape, 4095, jnp.int32)
     ids[:, : chosen.shape[1]] = chosen[...]
     turned = tokens[...].astype(F32).T
@@ -164,16 +172,6 @@
     return place(core, 2 * Y + b, 2 * X + a, ny, nx)
 
 
-def turn_kernel(ny, nx, core_ref, gate_ref, up_ref, out):
-    _, _, hid = gate_ref.shape
-    cells = ny * nx // 4
-    for s in range(4):
-        for half, ref in enumerate((gate_ref, up_ref)):
-            pieces = [ref[block_of(core_ref[0], s, g, ny, nx)] for g in range(cells)]
-            rows = jnp.concatenate(pieces, axis=0)
-            out[s, half * hid : (half + 1) * hid] = rows.T
-
-
 def turn_down_kernel(ny, nx, core_ref, corner_ref, down_ref, w0, w1, w2, w3, turned):
     tp, part, hid = turned.shape
     for y in range(ny):
@@ -190,7 +188,7 @@
         out[k] = array[...]
 
 
-def hidden_kernel(x_ref, w_ref, out, normed):
+def hidden_kernel(ny, nx, core_ref, x_ref, gate_ref, up_ref, out, normed):
     corners, depth, slots = x_ref.shape
     hid = out.shape[1]
     width = corners * depth
@@ -199,7 +197,9 @@
         v = x_ref[s].astype(F32)
         square += jnp.sum(v * v, axis=0, keepdims=True)
     scale = lax.rsqrt(square / width + EPS)
-    acc = jnp.zeros((2 * hid, slots), F32)
+    gate = jnp.zeros((hid, slots), F32)
+    up = jnp.zeros((hid, slots), F32)
+    dims = (((0,), (0,)), ((), ()))
     for s in range(corners):
         v = x_ref[s]
         parts = v[:, slots - 128 :].astype(F32)
@@ -207,8 +207,11 @@
         keep = (lane >= 120) & (lane < 123)
         gain = jnp.sum(jnp.where(keep, parts, 0.0), axis=1, keepdims=True)
         normed[...] = (v.astype(F32) * scale * gain).astype(BF16)
-        acc += jnp.dot(w_ref[s], normed[...], preferred_element_type=F32)
-    gate, up = acc[:hid], acc[hid:]
+        places = [block_of(core_ref[0], s, g, ny, nx) for g in range(ny * nx // 4)]
+        rows = jnp.concatenate([gate_ref[p] for p in places], axis=0)
+        gate += lax.dot_general(rows, normed[...], dims, preferred_element_type=F32)
+        rows = jnp.concatenate([up_ref[p] for p in places], axis=0)
+        up += lax.dot_general(rows, normed[...], dims, preferred_element_type=F32)
     value = (gate / (1.0 + jnp.exp(-gate)) * up).astype(BF16)
     for k in range(out.shape[0]):
         out[k] = value
@@ -276,6 +279,12 @@
             jax.ShapeDtypeStruct((1, SLOTS), jnp.int32),
         ],
         (tokens.T, chosen),
+        [pl.BlockSpec(memory_space=pltpu.HBM)] * 2,
+        [
+            pltpu.VMEM((part, tok_dev), BF16),
+            pltpu.VMEM(chosen.shape, jnp.int32),
+            pltpu.SemaphoreType.DMA((2,)),
+        ],
     )
     gathered = lax.all_to_all(packed, "z", 0, 0, tiled=True)
 
@@ -291,15 +300,6 @@
     for flip in range(1, 4):
         pairs = [(g[s], g[s ^ flip]) for g in near for s in range(4)]
         downs[flip] = lax.ppermute(downs[flip], PLANE, pairs)
-    turned = call(
-        functools.partial(turn_kernel, ny, nx),
-        jax.ShapeDtypeStruct((4, 2 * hid, cells * part), BF16),
-        (core, w_gate[0].reshape(tp, part, hid), w_up[0].reshape(tp, part, hid)),
-        [SMEM, VMEM, VMEM],
-        flops=1 << 30,
-    )
-    gathered, turned = lax.optimization_barrier((gathered, turned))
-
     swapped = lax.ppermute(gathered, "core", swap)
     own = call(
         functools.partial(pick_kernel, tok_dev),
@@ -308,6 +308,7 @@
         [SMEM] + [VMEM] * 3,
         flops=2 * part * nz * tok_dev * SLOTS,
     )
+    swapped, downs = lax.optimization_barrier((swapped, downs))
     picked = call(
         functools.partial(pick_other_kernel, tok_dev),
         jax.ShapeDtypeStruct((cells, part, SLOTS), BF16),
@@ -319,7 +320,6 @@
     column = lax.all_to_all(
         picked, PLANE, 0, 0, axis_index_groups=far, tiled=True
     ).reshape(cells * part, SLOTS)
-    column, downs = lax.optimization_barrier((column, downs))
     copies = call(
         copies_kernel,
         jax.ShapeDtypeStruct((4, cells * part, SLOTS), BF16),
@@ -328,9 +328,10 @@
     )
     full = lax.all_to_all(copies, PLANE, 0, 0, axis_index_groups=near, tiled=True)
     hidden = call(
-        hidden_kernel,
+        functools.partial(hidden_kernel, ny, nx),
         jax.ShapeDtypeStruct((4, hid, SLOTS), BF16),
-        (full, turned),
+        (core, full, w_gate[0].reshape(tp, part, hid), w_up[0].reshape(tp, part, hid)),
+        [SMEM] + [VMEM] * 3,
         scratch=[pltpu.VMEM((cells * part, SLOTS), BF16)],
         flops=4 * width * hid * SLOTS,
     )

time: 150 us -> 157 us (1.047)
  blocking collectives: 32.3 us -> 53.1 us
  starting transfers between devices: 51.4 us -> 41.5 us
  local copies, waits for them, and re-layouts: 7.25 us -> 2.68 us
  waiting for transfers between devices: 45.9 us -> 47.6 us
    all_to_all x0 -> x1, blocking collectives: none -> 20.2 us  [local(): lax.all_to_all(picked, PLANE, 0, 0, axis_index_groups=far, tiled=True)]
    all_to_all x1 -> x0, starting transfers between devices: 9.79 us -> none  [local(): lax.all_to_all(picked, PLANE, 0, 0, axis_index_groups=far, tiled=True)]
    unnamed x26 -> x14, local copies, waits for them, and re-layouts: 7.25 us -> 2.68 us
    all_to_all x1, waiting for transfers between devices: 12.6 us -> 15.7 us  [local(): gathered = lax.all_to_all(packed, 'z', 0, 0, tiled=True)]
    pallas_call x12 -> x11, Pallas kernels: 11.8 us -> 10.6 us  [call(): pl.pallas_call(kernel, out_shape=outs, in_specs=specs or [VMEM] * len(arg...]
  transfers between devices with their start and end apart: 8 -> 7, of which waited for: 6 -> 5; matrix products, arithmetic and copies ran while one was open for 0% -> 0% of each run, Pallas kernels for 3% -> 2%
where the time goes in v3:
time: 157 us; the launch traced here: 156 us
  blocking collectives  53.1 us (34%)
  waiting for transfers between devices  47.6 us (30%)
  starting transfers between devices  41.5 us (26%)
  Pallas kernels  10.6 us (7%)
  local copies, waits for them, and re-layouts  2.68 us (2%)
    all_to_all x1, blocking collectives, local(): lax.all_to_all(picked, PLANE, 0, 0, axis_index_groups=far, tiled=True)  20.2 us
    all_to_all x1, blocking collectives, local(): lax.all_to_all(copies, PLANE, 0, 0, axis_index_groups=near, tiled=True)  19.3 us
    all_to_all x1, starting transfers between devices, local(): gathered = lax.all_to_all(packed, 'z', 0, 0, tiled=True)  15.7 us
    all_to_all x1, waiting for transfers between devices, local(): gathered = lax.all_to_all(packed, 'z', 0, 0, tiled=True)  15.7 us
    all_to_all x1, blocking collectives, local(): lax.all_to_all(hidden, PLANE, 0, 0, axis_index_groups=near, tiled=True)  13.5 us
    all_to_all x1, waiting for transfers between devices, local(): lax.all_to_all(partial.reshape(cells, part, SLOTS), PLANE, 0, 0, axis_ind...  13.2 us
    ppermute x3, starting transfers between devices, local(): downs[flip] = lax.ppermute(downs[flip], PLANE, pairs)  11.4 us
    all_to_all x1, waiting for transfers between devices, local(): lax.all_to_all(sent.reshape(experts, SIDE, 128), ('z', 'core'), 0, 0, til...  11.2 us
  transfers between devices with their start and end apart: 7, of which 5 were waited for; matrix products, arithmetic and copies ran while one was open for 0% of the time, Pallas kernels for 2%

profile of v3, /device:TPU:1, one launch (start us, length us, event | category | flops | bytes accessed | tf_op | source)
XLA Modules:
  0.0 155.6 jit_solution(2026789905145519374)
XLA Ops:
  0.0 0.0 copy-start.2
  0.0 0.8 copy-done.2
  0.8 0.0 copy-start.3
  0.8 0.7 copy-done.3
  1.4 0.9 shard_map.73
  2.4 15.7 %all-to-all-start = ((bf16[12,96,128]{2,1,0:T(8,128)(2,1)}), bf16[12,96,128]{2,1,0:T(8,128)(2,1)S(1)}, u32[]{:S(2)}, u32[]{:S(2)}) async-start(bf16[12,96,128]{2,1,0:T(8,128)(2,1)} %get-tuple-element.24), calls=%async_computation | async-start | bytes 589824 | tf_op jit(solution)/shard_map/all_to_all | solution.py:289
  18.1 0.0 copy-start.6
  18.1 15.7 %all-to-all-done.gathered = bf16[12,96,128]{2,1,0:T(8,128)(2,1)S(1)} async-done(((bf16[12,96,128]{2,1,0:T(8,128)(2,1)}), bf16[12,96,128]{2,1,0:T(8,128)(2,1)S(1)}, u32[]{:S(2)}, u32[]{:S(2)}) %all-to-all-start) | async-done | bytes 294944 | tf_op jit(solution)/shard_map/all_to_all | solution.py:289
  33.8 4.1 %collective-permute-start = (bf16[12,96,128]{2,1,0:T(8,128)(2,1)S(1)}, bf16[12,96,128]{2,1,0:T(8,128)(2,1)S(1)}, u32[]{:S(2)}, u32[]{:S(2)}) collective-permute-start(bf16[12,96,128]{2,1,0:T(8,128)(2,1)S(1)} %all-to-all-done.gathered), channel_id=1, source_target_pairs={{0,32},{32,0},{1,33},{33,1},{2,34},{34,2},{3,35},{35,3},{4,36},{36... | collective-permute-start | bytes 884744 | tf_op jit(solution)/shard_map/ppermute | solution.py:303
  37.9 0.0 copy-start.5
  37.9 1.2 copy-done.5
  39.1 0.4 shard_map.74
  39.5 4.4 %collective-permute-start.1 = (bf16[512,256]{1,0:T(8,128)(2,1)S(1)}, bf16[512,256]{1,0:T(8,128)(2,1)S(1)}, u32[]{:S(2)}, u32[]{:S(2)}) collective-permute-start(bf16[512,256]{1,0:T(8,128)(2,1)S(1)} %get-tuple-element.26), channel_id=1, source_target_pairs={{0,1},{1,0},{4,5},{5,4},{2,3},{3,2},{6,7},{7,6},{8,9},{9,8},{12,13... | collective-permute-start | bytes 786440 | tf_op jit(solution)/shard_map/ppermute | solution.py:302
  43.9 5.1 %collective-permute-start.2 = (bf16[512,256]{1,0:T(8,128)(2,1)S(1)}, bf16[512,256]{1,0:T(8,128)(2,1)S(1)}, u32[]{:S(2)}, u32[]{:S(2)}) collective-permute-start(bf16[512,256]{1,0:T(8,128)(2,1)S(1)} %get-tuple-element.27), channel_id=1, source_target_pairs={{0,4},{1,5},{4,0},{5,1},{2,6},{3,7},{6,2},{7,3},{8,12},{9,13},{12,... | collective-permute-start | bytes 786440 | tf_op jit(solution)/shard_map/ppermute | solution.py:302
  49.0 1.9 %collective-permute-start.3 = (bf16[512,256]{1,0:T(8,128)(2,1)S(1)}, bf16[512,256]{1,0:T(8,128)(2,1)S(1)}, u32[]{:S(2)}, u32[]{:S(2)}) collective-permute-start(bf16[512,256]{1,0:T(8,128)(2,1)S(1)} %get-tuple-element.28), channel_id=1, source_target_pairs={{0,5},{1,4},{4,1},{5,0},{2,7},{3,6},{6,3},{7,2},{8,13},{9,12},{12,... | collective-permute-start | bytes 786440 | tf_op jit(solution)/shard_map/ppermute | solution.py:302
  50.9 0.0 copy-done.6
  51.0 0.9 shard_map.75.mine
  51.8 0.0 collective-permute-done.1.w1
  51.8 1.0 collective-permute-done.2.w2
  52.9 6.6 %collective-permute-done.3.w3 = bf16[512,256]{1,0:T(8,128)(2,1)S(1)} collective-permute-done((bf16[512,256]{1,0:T(8,128)(2,1)S(1)}, bf16[512,256]{1,0:T(8,128)(2,1)S(1)}, u32[]{:S(2)}, u32[]{:S(2)}) %collective-permute-start.3) | collective-permute-done | bytes 262176 | tf_op jit(solution)/shard_map/ppermute | solution.py:302
  59.4 0.0 collective-permute-done.swapped
  59.5 0.9 shard_map.76
  60.3 20.2 %all_to_all.30 = bf16[8,64,512]{2,1,0:T(8,128)(2,1)S(1)} all-to-all(bf16[8,64,512]{2,1,0:T(8,128)(2,1)S(1)} %shard_map.76), channel_id=1, replica_groups={{0,2,8,10,16,18,24,26},{1,3,9,11,17,19,25,27},{4,6,12,14,20,22,28,30},{..., dimensions={0} | all-to-all | bytes 1048576 | tf_op jit(solution)/shard_map/all_to_all | solution.py:320
  80.6 0.1 shard_map.77
  80.7 0.0 copy-start
  80.7 0.0 copy-start.1
  80.8 19.3 %all_to_all.31.x_ref = bf16[4,512,512]{2,1,0:T(8,128)(2,1)S(1)} all-to-all(bf16[4,512,512]{2,1,0:T(8,128)(2,1)S(1)} %shard_map.77), channel_id=1, replica_groups={{0,1,4,5},{2,3,6,7},{8,9,12,13},{10,11,14,15},{16,17,20,21},{18,19,22,2..., dimensions={0} | all-to-all | bytes 4194304 | tf_op jit(solution)/shard_map/all_to_all | solution.py:329
  100.1 0.0 copy-done
  100.1 0.0 copy-done.1
  100.1 1.6 %shard_map.78 = bf16[4,256,512]{2,1,0:T(8,128)(2,1)S(1)} custom-call(s32[1]{0:T(128)} %bitcast.1.core_ref, bf16[4,512,512]{2,1,0:T(8,128)(2,1)S(1)} %all_to_all.31.x_ref, bf16[32,64,256]{2,1,0:T(8,128)(2,1)S(1)} %bitcast.16, bf16[32,64,256]{2,1,0:T(8,128)(2,1)S(1)} %bitcast.17), custom_call_target="tpu_custom_call" | custom-call | flops 1073741824 | tf_op jit(solution)/shard_map/pallas_call | solution.py:23
  101.7 13.5 %all_to_all.32.hidden = bf16[4,256,512]{2,1,0:T(8,128)(2,1)S(1)} all-to-all(bf16[4,256,512]{2,1,0:T(8,128)(2,1)S(1)} %shard_map.78), channel_id=1, replica_groups={{0,1,4,5},{2,3,6,7},{8,9,12,13},{10,11,14,15},{16,17,20,21},{18,19,22,2..., dimensions={0} | all-to-all | bytes 2097152 | tf_op jit(solution)/shard_map/all_to_all | solution.py:338
  115.2 1.5 shard_map.79
  116.7 6.2 %all-to-all-start.4 = ((bf16[8,64,512]{2,1,0:T(8,128)(2,1)}), bf16[8,64,512]{2,1,0:T(8,128)(2,1)S(1)}, u32[]{:S(2)}, u32[]{:S(2)}) async-start(bf16[8,64,512]{2,1,0:T(8,128)(2,1)} %bitcast.8), calls=%async_computation.4 | async-start | bytes 1048576 | tf_op jit(solution)/shard_map/all_to_all | solution.py:348
  123.0 0.0 copy-start.4
  123.0 0.7 shard_map.80
  123.7 13.2 %all-to-all-done.4.arrived = bf16[8,64,512]{2,1,0:T(8,128)(2,1)S(1)} async-done(((bf16[8,64,512]{2,1,0:T(8,128)(2,1)}), bf16[8,64,512]{2,1,0:T(8,128)(2,1)S(1)}, u32[]{:S(2)}, u32[]{:S(2)}) %all-to-all-start.4) | async-done | bytes 524320 | tf_op jit(solution)/shard_map/all_to_all | solution.py:348
  136.9 0.0 copy-done.4
  136.9 1.1 shard_map.81
  138.0 4.0 %all-to-all-start.5 = ((bf16[24,24,128]{2,1,0:T(8,128)(2,1)}), bf16[24,24,128]{2,1,0:T(8,128)(2,1)S(1)}, u32[]{:S(2)}, u32[]{:S(2)}) async-start(bf16[24,24,128]{2,1,0:T(8,128)(2,1)} %bitcast.11), calls=%async_computation.5 | async-start | bytes 294912 | tf_op jit(solution)/shard_map/all_to_all | solution.py:374
  142.0 1.3 shard_map.82
  143.4 11.2 %all-to-all-done.5 = bf16[24,24,128]{2,1,0:T(8,128)(2,1)S(1)} async-done(((bf16[24,24,128]{2,1,0:T(8,128)(2,1)}), bf16[24,24,128]{2,1,0:T(8,128)(2,1)S(1)}, u32[]{:S(2)}, u32[]{:S(2)}) %all-to-all-start.5) | async-done | bytes 147488 | tf_op jit(solution)/shard_map/all_to_all | solution.py:374
  154.5 1.1 shard_map.83
Async XLA Ops:
  0.0 0.8 copy-start.2
  0.8 0.7 copy-start.3
  2.4 31.4 %all-to-all-start = ((bf16[12,96,128]{2,1,0:T(8,128)(2,1)}), bf16[12,96,128]{2,1,0:T(8,128)(2,1)S(1)}, u32[]{:S(2)}, u32[]{:S(2)}) async-start(bf16[12,96,128]{2,1,0:T(8,128)(2,1)} %get-tuple-element.24), calls=%async_computation | async-start | bytes 589824 | tf_op jit(solution)/shard_map/all_to_all | solution.py:289
  18.1 32.9 %copy-start.6 = (f32[64]{0:T(128)S(1)}, f32[64]{0:T(128)}, u32[]{:S(2)}) copy-start(f32[64]{0:T(128)} %param.8) | copy-start | bytes 772
  33.8 25.7 %collective-permute-start = (bf16[12,96,128]{2,1,0:T(8,128)(2,1)S(1)}, bf16[12,96,128]{2,1,0:T(8,128)(2,1)S(1)}, u32[]{:S(2)}, u32[]{:S(2)}) collective-permute-start(bf16[12,96,128]{2,1,0:T(8,128)(2,1)S(1)} %all-to-all-done.gathered), channel_id=1, source_target_pairs={{0,32},{32,0},{1,33},{33,1},{2,34},{34,2},{3,35},{35,3},{4,36},{36... | collective-permute-start | bytes 884744 | tf_op jit(solution)/shard_map/ppermute | solution.py:303
  37.9 1.2 copy-start.5
  39.5 12.3 %collective-permute-start.1 = (bf16[512,256]{1,0:T(8,128)(2,1)S(1)}, bf16[512,256]{1,0:T(8,128)(2,1)S(1)}, u32[]{:S(2)}, u32[]{:S(2)}) collective-permute-start(bf16[512,256]{1,0:T(8,128)(2,1)S(1)} %get-tuple-element.26), channel_id=1, source_target_pairs={{0,1},{1,0},{4,5},{5,4},{2,3},{3,2},{6,7},{7,6},{8,9},{9,8},{12,13... | collective-permute-start | bytes 786440 | tf_op jit(solution)/shard_map/ppermute | solution.py:302
  43.9 9.0 %collective-permute-start.2 = (bf16[512,256]{1,0:T(8,128)(2,1)S(1)}, bf16[512,256]{1,0:T(8,128)(2,1)S(1)}, u32[]{:S(2)}, u32[]{:S(2)}) collective-permute-start(bf16[512,256]{1,0:T(8,128)(2,1)S(1)} %get-tuple-element.27), channel_id=1, source_target_pairs={{0,4},{1,5},{4,0},{5,1},{2,6},{3,7},{6,2},{7,3},{8,12},{9,13},{12,... | collective-permute-start | bytes 786440 | tf_op jit(solution)/shard_map/ppermute | solution.py:302
  49.0 10.4 %collective-permute-start.3 = (bf16[512,256]{1,0:T(8,128)(2,1)S(1)}, bf16[512,256]{1,0:T(8,128)(2,1)S(1)}, u32[]{:S(2)}, u32[]{:S(2)}) collective-permute-start(bf16[512,256]{1,0:T(8,128)(2,1)S(1)} %get-tuple-element.28), channel_id=1, source_target_pairs={{0,5},{1,4},{4,1},{5,0},{2,7},{3,6},{6,3},{7,2},{8,13},{9,12},{12,... | collective-permute-start | bytes 786440 | tf_op jit(solution)/shard_map/ppermute | solution.py:302
  80.7 19.4 %copy-start = (bf16[1,2048,256]{2,1,0:T(8,128)(2,1)S(1)}, bf16[1,2048,256]{2,1,0:T(8,128)(2,1)}, u32[]{:S(2)}) copy-start(bf16[1,2048,256]{2,1,0:T(8,128)(2,1)} %param.11) | copy-start | bytes 3145732
  80.7 19.3 %copy-start.1 = (bf16[1,2048,256]{2,1,0:T(8,128)(2,1)S(1)}, bf16[1,2048,256]{2,1,0:T(8,128)(2,1)}, u32[]{:S(2)}) copy-start(bf16[1,2048,256]{2,1,0:T(8,128)(2,1)} %param.12) | copy-start | bytes 3145732
  116.7 20.1 %all-to-all-start.4 = ((bf16[8,64,512]{2,1,0:T(8,128)(2,1)}), bf16[8,64,512]{2,1,0:T(8,128)(2,1)S(1)}, u32[]{:S(2)}, u32[]{:S(2)}) async-start(bf16[8,64,512]{2,1,0:T(8,128)(2,1)} %bitcast.8), calls=%async_computation.4 | async-start | bytes 1048576 | tf_op jit(solution)/shard_map/all_to_all | solution.py:348
  123.0 13.9 %copy-start.4 = (f32[1,504]{1,0:T(1,128)S(1)}, f32[1,504]{1,0:T(1,128)}, u32[]{:S(2)}) copy-start(f32[1,504]{1,0:T(1,128)} %affinity.1) | copy-start | bytes 6052
  138.0 16.6 %all-to-all-start.5 = ((bf16[24,24,128]{2,1,0:T(8,128)(2,1)}), bf16[24,24,128]{2,1,0:T(8,128)(2,1)S(1)}, u32[]{:S(2)}, u32[]{:S(2)}) async-start(bf16[24,24,128]{2,1,0:T(8,128)(2,1)} %bitcast.11), calls=%async_computation.5 | async-start | bytes 294912 | tf_op jit(solution)/shard_map/all_to_all | solution.py:374

commit v4 on v3

--- a/solution.py
+++ b/solution.py
@@ -12,6 +12,8 @@
 SLOTS = 512
 HALF = 88
 SIDE = 24
+USED = 21
+NONE = 255.0
 VMEM = pl.BlockSpec(memory_space=pltpu.VMEM)
 SMEM = pl.BlockSpec(memory_space=pltpu.SMEM)
 BF16 = jnp.bfloat16
@@ -55,43 +57,41 @@
     return jnp.where(row == ids - base, 1.0, 0.0).astype(BF16)
 
 
-def pack_kernel(tokens_ref, chosen_ref, out, ids, tokens, chosen, sems):
+def pack_kernel(tokens, out):
     copies, part = out.shape[0], tokens.shape[0]
-    loads = [
-        pltpu.make_async_copy(tokens_ref, tokens, sems.at[0]),
-        pltpu.make_async_copy(chosen_ref, chosen, sems.at[1]),
-    ]
-    for load in loads:
-        load.start()
-    for load in loads:
-        load.wait()
-    ids[...] = jnp.full(ids.shape, 4095, jnp.int32)
-    ids[:, : chosen.shape[1]] = chosen[...]
     turned = tokens[...].astype(F32).T
     rest = turned.shape[0] - HALF
     upper = jnp.concatenate([turned[HALF:], jnp.zeros((HALF - rest, part), F32)], axis=0)
     rows = jnp.concatenate([turned[:HALF], upper], axis=1)
-    high = (ids[...] >> 6).astype(F32)
-    low = (ids[...] & 63).astype(F32)
-    lists = [v[:, k : k + 128] for v in (high, low) for k in range(0, SLOTS, 128)]
-    body = jnp.concatenate([rows, *lists], axis=0).astype(BF16)
+    body = rows.astype(BF16)
     for k in range(copies):
         out[k] = body
 
 
-def send_hot_kernel(tok_dev, ids, low, high):
+def send_hot_kernel(tok_dev, chosen, ids, low, high, extra):
     side = ids.shape[1]
+    ids[...] = jnp.full(ids.shape, 4095, jnp.int32)
+    ids[:, : chosen.shape[1]] = chosen[...]
     token = ids[...].astype(F32)
     owner = jnp.floor((token + 0.5) * (1.0 / tok_dev))
+    local = token - owner * tok_dev
     column = jnp.broadcast_to(token, (128, side)).T[:, :1]
     column_owner = jnp.broadcast_to(owner, (128, side)).T[:, :1]
     before = (column < token) & (column_owner == owner)
     rank = jnp.sum(jnp.where(before, 1.0, 0.0), axis=0, keepdims=True)
-    code = (owner * (2.0 * SIDE) + rank).astype(jnp.int32)
+    code = (owner * (2.0 * USED) + rank).astype(jnp.int32)
     row = lax.broadcasted_iota(jnp.int32, (SIDE, side), 0)
+    slot = lax.broadcasted_iota(jnp.int32, (SIDE, 128), 0)
+    lane = lax.broadcasted_iota(jnp.int32, (SIDE, 128), 1)
     for o in range(low.shape[0]):
-        low[o] = jnp.where(code == row + 2 * SIDE * o, 1.0, 0.0).astype(BF16)
-        high[o] = jnp.where(code == row + 2 * SIDE * o + SIDE, 1.0, 0.0).astype(BF16)
+        named = jnp.zeros((SIDE, 128), F32)
+        for half, ref in enumerate((low, high)):
+            match = (code == row + (2 * o + half) * USED) & (row < USED)
+            ref[o] = jnp.where(match, 1.0, 0.0).astype(BF16)
+            name = jnp.sum(jnp.where(match, local - NONE, 0.0), axis=1, keepdims=True)
+            line = jnp.sum(jnp.where(slot == lane, name, 0.0), axis=0, keepdims=True) + NONE
+            named = jnp.where(slot == USED + half, line, named)
+        extra[o] = named
 
 
 def pick(tok_dev, core, gathered, ids, part):
@@ -127,43 +127,6 @@
     total = (acc + mine[...]).astype(BF16)
     for g in range(out.shape[0]):
         out[g] = total
-
-
-def member_kernel(plane_ref, core_ref, gathered, swapped, low, high):
-    blocks = gathered.shape[0]
-    tokens = low.shape[0]
-    core = core_ref[0]
-    base = (2 * plane_ref[0] + core) * tokens
-    token = (lax.broadcasted_iota(jnp.int32, (tokens, 128), 0) + base).astype(F32)
-    expert = lax.broadcasted_iota(jnp.int32, (tokens, 128), 1)
-    member = jnp.zeros((tokens, 128), F32)
-    for source in range(2):
-        for b in range(blocks):
-            lists = (gathered, swapped)[source][b, HALF : HALF + 8, :].astype(F32)
-            ids = lists[:4] * 64.0 + lists[4:]
-            found = jnp.zeros((tokens, 128), F32)
-            for k in range(4):
-                found += jnp.where(token == ids[k : k + 1], 1.0, 0.0)
-            count = jnp.sum(found, axis=1, keepdims=True)
-            which = 2 * b + (core if source == 0 else 1 - core)
-            member += jnp.where(expert == which, count, 0.0)
-    triangle = (tokens, tokens)
-    earlier = lax.broadcasted_iota(jnp.int32, triangle, 1) < lax.broadcasted_iota(
-        jnp.int32, triangle, 0
-    )
-    rank = jnp.dot(
-        jnp.where(earlier, 1.0, 0.0).astype(BF16), member.astype(BF16), preferred_element_type=F32
-    )
-    slot = jnp.where(member > 0.5, rank, 255.0).astype(BF16)
-    spread = (128, low.shape[1])
-    line = lax.broadcasted_iota(jnp.int32, spread, 0) * SIDE
-    place = lax.broadcasted_iota(jnp.int32, spread, 1)
-    inside = (place >= line) & (place < line + SIDE)
-    slots = jnp.dot(slot, jnp.where(inside, 1.0, 0.0).astype(BF16), preferred_element_type=F32)
-    start = jnp.zeros(spread, jnp.int32) + jnp.where(inside, place - line, 0)
-    start = jnp.sum(start.astype(F32), axis=0, keepdims=True)
-    low[...] = jnp.where(slots == start, 1.0, 0.0).astype(BF16)
-    high[...] = jnp.where(slots == start + float(SIDE), 1.0, 0.0).astype(BF16)
 
 
 def block_of(core, corner, cell, ny, nx):
@@ -225,7 +188,7 @@
     out[...] = acc.astype(BF16)
 
 
-def send_kernel(arrived, affinity, low, high, out, weight):
+def send_kernel(arrived, affinity, low, high, extra, out, weight):
     weight[...] = jnp.zeros(weight.shape, F32)
     weight[:, : affinity.shape[1]] = affinity[...]
     total = arrived[0].astype(F32)
@@ -246,14 +209,28 @@
         dims,
         preferred_element_type=F32,
     )
-    out[...] = rows.astype(BF16)
-
-
-def final_kernel(arrived, low, high, out):
-    part = out.shape[0]
-    total = jnp.dot(low[...], arrived[...], preferred_element_type=F32)[:, :part]
-    total += jnp.dot(high[...], arrived[...], preferred_element_type=F32)[:, part:]
-    out[...] = total.T.astype(BF16)
+    out[...] = (rows + extra[...]).astype(BF16)
+
+
+def final_kernel(arrived, out):
+    part, tokens = out.shape
+    experts = arrived.shape[0]
+    slot = lax.broadcasted_iota(jnp.int32, (SIDE, 128), 0)
+    lane = lax.broadcasted_iota(jnp.int32, (SIDE, 128), 1)
+    token = lax.broadcasted_iota(jnp.int32, (SIDE, tokens), 1).astype(F32)
+    hots = ([], [])
+    for e in range(experts):
+        block = arrived[e].astype(F32)
+        for half in range(2):
+            line = block[USED + half : USED + half + 1]
+            name = jnp.sum(jnp.where(slot == lane, line, 0.0), axis=1, keepdims=True)
+            hots[half].append(jnp.where(token == name, 1.0, 0.0))
+    rows = arrived[...].reshape(experts * SIDE, 128)
+    dims = (((0,), (0,)), ((), ()))
+    low, high = (jnp.concatenate(h, axis=0).astype(BF16) for h in hots)
+    total = lax.dot_general(rows, low, dims, preferred_element_type=F32)[:part]
+    total += lax.dot_general(rows, high, dims, preferred_element_type=F32)[part:]
+    out[...] = total.astype(BF16)
 
 
 def local(tokens, norm_gain, chosen, affinity, w_gate, w_up, w_down):
@@ -265,26 +242,15 @@
     near, far = tiles(ny, nx)
     swap = [(0, 1), (1, 0)]
     core_index = lax.axis_index("core").astype(jnp.int32)
-    z_index = lax.axis_index("z").astype(jnp.int32)
     y_index = lax.axis_index("y").astype(jnp.int32)
     x_index = lax.axis_index("x").astype(jnp.int32)
     corner_index = ((y_index + core_index) & 1) * 2 + ((x_index + core_index) & 1)
     core, corner = core_index.reshape(1), corner_index.reshape(1)
-    plane = z_index.reshape(1)
-
-    packed, own_ids = call(
+
+    packed = call(
         pack_kernel,
-        [
-            jax.ShapeDtypeStruct((nz, HALF + 8, 128), BF16),
-            jax.ShapeDtypeStruct((1, SLOTS), jnp.int32),
-        ],
-        (tokens.T, chosen),
-        [pl.BlockSpec(memory_space=pltpu.HBM)] * 2,
-        [
-            pltpu.VMEM((part, tok_dev), BF16),
-            pltpu.VMEM(chosen.shape, jnp.int32),
-            pltpu.SemaphoreType.DMA((2,)),
-        ],
+        jax.ShapeDtypeStruct((nz, HALF, 128), BF16),
+        (tokens.T,),
     )
     gathered = lax.all_to_all(packed, "z", 0, 0, tiled=True)
 
@@ -300,6 +266,19 @@
     for flip in range(1, 4):
         pairs = [(g[s], g[s ^ flip]) for g in near for s in range(4)]
         downs[flip] = lax.ppermute(downs[flip], PLANE, pairs)
+    hot_shape = jax.ShapeDtypeStruct((experts, SIDE, SLOTS), BF16)
+    own_ids, *send_hot = call(
+        functools.partial(send_hot_kernel, tok_dev),
+        [
+            jax.ShapeDtypeStruct((1, SLOTS), jnp.int32),
+            hot_shape,
+            hot_shape,
+            jax.ShapeDtypeStruct((experts, SIDE, 128), F32),
+        ],
+        (chosen,),
+        flops=1 << 30,
+    )
+    send_hot = [v.reshape(experts * SIDE, -1) for v in send_hot]
     swapped = lax.ppermute(gathered, "core", swap)
     own = call(
         functools.partial(pick_kernel, tok_dev),
@@ -343,26 +322,8 @@
         [SMEM] + [VMEM] * 5,
         flops=2 * width * hid * SLOTS,
     )
-    late = lax.optimization_barrier((partial, own_ids, gathered, swapped))
-    partial, own_ids, gathered, swapped = late
     arrived = lax.all_to_all(
         partial.reshape(cells, part, SLOTS), PLANE, 0, 0, axis_index_groups=far, tiled=True
-    )
-    hot_shape = jax.ShapeDtypeStruct((experts, SIDE, SLOTS), BF16)
-    send_hot = call(
-        functools.partial(send_hot_kernel, tok_dev),
-        [hot_shape, hot_shape],
-        (own_ids,),
-        flops=1 << 30,
-    )
-    send_hot = [v.reshape(experts * SIDE, SLOTS) for v in send_hot]
-    hot_shape = jax.ShapeDtypeStruct((tok_dev, experts * SIDE), BF16)
-    final_hot = call(
-        member_kernel,
-        [hot_shape, hot_shape],
-        (plane, core, gathered, swapped),
-        [SMEM, SMEM, VMEM, VMEM],
-        flops=1 << 31,
     )
     sent = call(
         send_kernel,
@@ -371,13 +332,11 @@
         scratch=[pltpu.VMEM((1, SLOTS), F32)],
         flops=4 * 128 * experts * SIDE * SLOTS,
     )
-    back = lax.all_to_all(
-        sent.reshape(experts, SIDE, 128), ("z", "core"), 0, 0, tiled=True
-    ).reshape(experts * SIDE, 128)
+    back = lax.all_to_all(sent.reshape(experts, SIDE, 128), ("z", "core"), 0, 0, tiled=True)
     total = call(
         final_kernel,
         jax.ShapeDtypeStruct((part, tok_dev), BF16),
-        (back, *final_hot),
+        (back,),
         flops=4 * 128 * experts * SIDE * tok_dev,
     )
     return total.T

time: 157 us -> 154 us (0.981)
  blocking collectives: 53.1 us -> 89.6 us
  waiting for transfers between devices: 47.6 us -> 21.3 us
  starting transfers between devices: 41.5 us -> 31.5 us
  Pallas kernels: 10.6 us -> 8.09 us
    all_to_all x0 -> x2, blocking collectives: none -> 36.5 us  [the longest x1 20.6 us: local(): lax.all_to_all(partial.reshape(cells, part, SLOTS), PLANE, 0, 0, axis_ind...]
    all_to_all x2 -> x0, waiting for transfers between devices: 24.3 us -> none  [the longest x1 13.2 us: local(): lax.all_to_all(partial.reshape(cells, part, SLOTS), PLANE, 0, 0, axis_ind...]
    all_to_all x2 -> x0, starting transfers between devices: 10.3 us -> none  [the longest x1 6.23 us: local(): lax.all_to_all(partial.reshape(cells, part, SLOTS), PLANE, 0, 0, axis_ind...]
    pallas_call x11 -> x10, Pallas kernels: 10.6 us -> 8.09 us  [call(): pl.pallas_call(kernel, out_shape=outs, in_specs=specs or [VMEM] * len(arg...]
  transfers between devices with their start and end apart: 7 -> 5, of which waited for: 5 -> 3; matrix products, arithmetic and copies ran while one was open for 0% -> 0% of each run, Pallas kernels for 2% -> 1%
where the time goes in v4:
time: 154 us; the launch traced here: 153 us
  blocking collectives  89.6 us (58%)
  starting transfers between devices  31.5 us (20%)
  waiting for transfers between devices  21.3 us (14%)
  Pallas kernels  8.09 us (5%)
  local copies, waits for them, and re-layouts  2.01 us (1%)
    all_to_all x1, blocking collectives, local(): lax.all_to_all(partial.reshape(cells, part, SLOTS), PLANE, 0, 0, axis_ind...  20.6 us
    all_to_all x1, blocking collectives, local(): lax.all_to_all(picked, PLANE, 0, 0, axis_index_groups=far, tiled=True)  20.2 us
    all_to_all x1, blocking collectives, local(): lax.all_to_all(copies, PLANE, 0, 0, axis_index_groups=near, tiled=True)  19.3 us
    all_to_all x1, blocking collectives, local(): lax.all_to_all(sent.reshape(experts, SIDE, 128), ('z', 'core'), 0, 0, til...  15.9 us
    all_to_all x1, starting transfers between devices, local(): gathered = lax.all_to_all(packed, 'z', 0, 0, tiled=True)  15.7 us
    all_to_all x1, waiting for transfers between devices, local(): gathered = lax.all_to_all(packed, 'z', 0, 0, tiled=True)  14.6 us
    all_to_all x1, blocking collectives, local(): lax.all_to_all(hidden, PLANE, 0, 0, axis_index_groups=near, tiled=True)  13.5 us
    ppermute x3, starting transfers between devices, local(): downs[flip] = lax.ppermute(downs[flip], PLANE, pairs)  11.4 us
  transfers between devices with their start and end apart: 5, of which 3 were waited for; matrix products, arithmetic and copies ran while one was open for 0% of the time, Pallas kernels for 1%

profile of v4, /device:TPU:1, one launch (start us, length us, event | category | flops | bytes accessed | tf_op | source)
XLA Modules:
  0.0 152.7 jit_solution(1480865141109145099)
XLA Ops:
  0.0 0.0 copy-start.2
  0.0 0.8 copy-done.2
  0.8 0.9 shard_map.73
  1.6 15.7 %all-to-all-start = ((bf16[12,88,128]{2,1,0:T(8,128)(2,1)}), bf16[12,88,128]{2,1,0:T(8,128)(2,1)S(1)}, u32[]{:S(2)}, u32[]{:S(2)}) async-start(bf16[12,88,128]{2,1,0:T(8,128)(2,1)} %shard_map.73), calls=%async_computation | async-start | bytes 540672 | tf_op jit(solution)/shard_map/all_to_all | solution.py:255
  17.3 0.0 copy-start.5
  17.4 14.6 %all-to-all-done.gathered = bf16[12,88,128]{2,1,0:T(8,128)(2,1)S(1)} async-done(((bf16[12,88,128]{2,1,0:T(8,128)(2,1)}), bf16[12,88,128]{2,1,0:T(8,128)(2,1)S(1)}, u32[]{:S(2)}, u32[]{:S(2)}) %all-to-all-start) | async-done | bytes 270368 | tf_op jit(solution)/shard_map/all_to_all | solution.py:255
  32.0 4.4 %collective-permute-start = (bf16[12,88,128]{2,1,0:T(8,128)(2,1)S(1)}, bf16[12,88,128]{2,1,0:T(8,128)(2,1)S(1)}, u32[]{:S(2)}, u32[]{:S(2)}) collective-permute-start(bf16[12,88,128]{2,1,0:T(8,128)(2,1)S(1)} %all-to-all-done.gathered), channel_id=1, source_target_pairs={{0,32},{32,0},{1,33},{33,1},{2,34},{34,2},{3,35},{35,3},{4,36},{36... | collective-permute-start | bytes 811016 | tf_op jit(solution)/shard_map/ppermute | solution.py:282
  36.4 0.0 copy-start.4
  36.5 1.2 copy-done.4
  37.7 0.4 shard_map.74
  38.1 0.0 copy-start.6
  38.1 4.4 %collective-permute-start.1 = (bf16[512,256]{1,0:T(8,128)(2,1)S(1)}, bf16[512,256]{1,0:T(8,128)(2,1)S(1)}, u32[]{:S(2)}, u32[]{:S(2)}) collective-permute-start(bf16[512,256]{1,0:T(8,128)(2,1)S(1)} %get-tuple-element.19), channel_id=1, source_target_pairs={{0,1},{1,0},{4,5},{5,4},{2,3},{3,2},{6,7},{7,6},{8,9},{9,8},{12,13... | collective-permute-start | bytes 786440 | tf_op jit(solution)/shard_map/ppermute | solution.py:268
  42.5 5.1 %collective-permute-start.2 = (bf16[512,256]{1,0:T(8,128)(2,1)S(1)}, bf16[512,256]{1,0:T(8,128)(2,1)S(1)}, u32[]{:S(2)}, u32[]{:S(2)}) collective-permute-start(bf16[512,256]{1,0:T(8,128)(2,1)S(1)} %get-tuple-element.20), channel_id=1, source_target_pairs={{0,4},{1,5},{4,0},{5,1},{2,6},{3,7},{6,2},{7,3},{8,12},{9,13},{12,... | collective-permute-start | bytes 786440 | tf_op jit(solution)/shard_map/ppermute | solution.py:268
  47.6 1.9 %collective-permute-start.3 = (bf16[512,256]{1,0:T(8,128)(2,1)S(1)}, bf16[512,256]{1,0:T(8,128)(2,1)S(1)}, u32[]{:S(2)}, u32[]{:S(2)}) collective-permute-start(bf16[512,256]{1,0:T(8,128)(2,1)S(1)} %get-tuple-element.21), channel_id=1, source_target_pairs={{0,5},{1,4},{4,1},{5,0},{2,7},{3,6},{6,3},{7,2},{8,13},{9,12},{12,... | collective-permute-start | bytes 786440 | tf_op jit(solution)/shard_map/ppermute | solution.py:268
  49.5 0.0 copy-done.5
  49.5 0.9 shard_map.75
  50.5 0.0 copy-done.6
  50.5 0.9 shard_map.76.mine
  51.4 0.0 collective-permute-done.1.w1
  51.4 0.1 collective-permute-done.2.w2
  51.5 6.6 %collective-permute-done.3.w3 = bf16[512,256]{1,0:T(8,128)(2,1)S(1)} collective-permute-done((bf16[512,256]{1,0:T(8,128)(2,1)S(1)}, bf16[512,256]{1,0:T(8,128)(2,1)S(1)}, u32[]{:S(2)}, u32[]{:S(2)}) %collective-permute-start.3) | collective-permute-done | bytes 262176 | tf_op jit(solution)/shard_map/ppermute | solution.py:268
  58.0 0.0 collective-permute-done.swapped
  58.0 0.9 shard_map.77
  58.9 20.2 %all_to_all.30 = bf16[8,64,512]{2,1,0:T(8,128)(2,1)S(1)} all-to-all(bf16[8,64,512]{2,1,0:T(8,128)(2,1)S(1)} %shard_map.77), channel_id=1, replica_groups={{0,2,8,10,16,18,24,26},{1,3,9,11,17,19,25,27},{4,6,12,14,20,22,28,30},{..., dimensions={0} | all-to-all | bytes 1048576 | tf_op jit(solution)/shard_map/all_to_all | solution.py:299
  79.2 0.1 shard_map.78
  79.3 0.0 copy-start
  79.3 0.0 copy-start.1
  79.3 19.3 %all_to_all.31.x_ref = bf16[4,512,512]{2,1,0:T(8,128)(2,1)S(1)} all-to-all(bf16[4,512,512]{2,1,0:T(8,128)(2,1)S(1)} %shard_map.78), channel_id=1, replica_groups={{0,1,4,5},{2,3,6,7},{8,9,12,13},{10,11,14,15},{16,17,20,21},{18,19,22,2..., dimensions={0} | all-to-all | bytes 4194304 | tf_op jit(solution)/shard_map/all_to_all | solution.py:308
  98.7 0.0 copy-done
  98.7 0.0 copy-done.1
  98.7 1.7 %shard_map.79 = bf16[4,256,512]{2,1,0:T(8,128)(2,1)S(1)} custom-call(s32[1]{0:T(128)} %bitcast.1.core_ref, bf16[4,512,512]{2,1,0:T(8,128)(2,1)S(1)} %all_to_all.31.x_ref, bf16[32,64,256]{2,1,0:T(8,128)(2,1)S(1)} %bitcast.16, bf16[32,64,256]{2,1,0:T(8,128)(2,1)S(1)} %bitcast.17), custom_call_target="tpu_custom_call" | custom-call | flops 1073741824 | tf_op jit(solution)/shard_map/pallas_call | solution.py:25
  100.3 13.5 %all_to_all.32.hidden = bf16[4,256,512]{2,1,0:T(8,128)(2,1)S(1)} all-to-all(bf16[4,256,512]{2,1,0:T(8,128)(2,1)S(1)} %shard_map.79), channel_id=1, replica_groups={{0,1,4,5},{2,3,6,7},{8,9,12,13},{10,11,14,15},{16,17,20,21},{18,19,22,2..., dimensions={0} | all-to-all | bytes 2097152 | tf_op jit(solution)/shard_map/all_to_all | solution.py:317
  113.8 0.0 copy-start.3
  113.8 0.7 shard_map.80
  114.5 20.6 %all_to_all.33.arrived = bf16[8,64,512]{2,1,0:T(8,128)(2,1)S(1)} all-to-all(bf16[8,64,512]{2,1,0:T(8,128)(2,1)S(1)} %bitcast.15), channel_id=1, replica_groups={{0,2,8,10,16,18,24,26},{1,3,9,11,17,19,25,27},{4,6,12,14,20,22,28,30},{..., dimensions={0} | all-to-all | bytes 1048576 | tf_op jit(solution)/shard_map/all_to_all | solution.py:325
  135.2 0.0 copy-done.3
  135.2 0.5 shard_map.81
  135.7 15.9 %all_to_all.34.arrived = bf16[24,24,128]{2,1,0:T(8,128)(2,1)S(1)} all-to-all(bf16[24,24,128]{2,1,0:T(8,128)(2,1)S(1)} %bitcast.18), channel_id=1, replica_groups=mesh['z'=12,'core'=2,'y'=8,'x'=4] {'z','core'}, dimensions={0} | all-to-all | bytes 294912 | tf_op jit(solution)/shard_map/all_to_all | solution.py:335
  151.6 1.1 shard_map.82
Async XLA Ops:
  0.0 0.8 copy-start.2
  1.6 30.3 %all-to-all-start = ((bf16[12,88,128]{2,1,0:T(8,128)(2,1)}), bf16[12,88,128]{2,1,0:T(8,128)(2,1)S(1)}, u32[]{:S(2)}, u32[]{:S(2)}) async-start(bf16[12,88,128]{2,1,0:T(8,128)(2,1)} %shard_map.73), calls=%async_computation | async-start | bytes 540672 | tf_op jit(solution)/shard_map/all_to_all | solution.py:255
  17.3 32.2 %copy-start.5 = (s32[1,504]{1,0:T(1,128)S(1)}, s32[1,504]{1,0:T(1,128)}, u32[]{:S(2)}) copy-start(s32[1,504]{1,0:T(1,128)} %chosen.1) | copy-start | bytes 6052
  32.0 26.0 %collective-permute-start = (bf16[12,88,128]{2,1,0:T(8,128)(2,1)S(1)}, bf16[12,88,128]{2,1,0:T(8,128)(2,1)S(1)}, u32[]{:S(2)}, u32[]{:S(2)}) collective-permute-start(bf16[12,88,128]{2,1,0:T(8,128)(2,1)S(1)} %all-to-all-done.gathered), channel_id=1, source_target_pairs={{0,32},{32,0},{1,33},{33,1},{2,34},{34,2},{3,35},{35,3},{4,36},{36... | collective-permute-start | bytes 811016 | tf_op jit(solution)/shard_map/ppermute | solution.py:282
  36.4 1.2 copy-start.4
  38.1 12.4 %copy-start.6 = (f32[64]{0:T(128)S(1)}, f32[64]{0:T(128)}, u32[]{:S(2)}) copy-start(f32[64]{0:T(128)} %param.8) | copy-start | bytes 772
  38.1 13.3 %collective-permute-start.1 = (bf16[512,256]{1,0:T(8,128)(2,1)S(1)}, bf16[512,256]{1,0:T(8,128)(2,1)S(1)}, u32[]{:S(2)}, u32[]{:S(2)}) collective-permute-start(bf16[512,256]{1,0:T(8,128)(2,1)S(1)} %get-tuple-element.19), channel_id=1, source_target_pairs={{0,1},{1,0},{4,5},{5,4},{2,3},{3,2},{6,7},{7,6},{8,9},{9,8},{12,13... | collective-permute-start | bytes 786440 | tf_op jit(solution)/shard_map/ppermute | solution.py:268
  42.5 9.0 %collective-permute-start.2 = (bf16[512,256]{1,0:T(8,128)(2,1)S(1)}, bf16[512,256]{1,0:T(8,128)(2,1)S(1)}, u32[]{:S(2)}, u32[]{:S(2)}) collective-permute-start(bf16[512,256]{1,0:T(8,128)(2,1)S(1)} %get-tuple-element.20), channel_id=1, source_target_pairs={{0,4},{1,5},{4,0},{5,1},{2,6},{3,7},{6,2},{7,3},{8,12},{9,13},{12,... | collective-permute-start | bytes 786440 | tf_op jit(solution)/shard_map/ppermute | solution.py:268
  47.6 10.4 %collective-permute-start.3 = (bf16[512,256]{1,0:T(8,128)(2,1)S(1)}, bf16[512,256]{1,0:T(8,128)(2,1)S(1)}, u32[]{:S(2)}, u32[]{:S(2)}) collective-permute-start(bf16[512,256]{1,0:T(8,128)(2,1)S(1)} %get-tuple-element.21), channel_id=1, source_target_pairs={{0,5},{1,4},{4,1},{5,0},{2,7},{3,6},{6,3},{7,2},{8,13},{9,12},{12,... | collective-permute-start | bytes 786440 | tf_op jit(solution)/shard_map/ppermute | solution.py:268
  79.3 19.4 %copy-start = (bf16[1,2048,256]{2,1,0:T(8,128)(2,1)S(1)}, bf16[1,2048,256]{2,1,0:T(8,128)(2,1)}, u32[]{:S(2)}) copy-start(bf16[1,2048,256]{2,1,0:T(8,128)(2,1)} %param.11) | copy-start | bytes 3145732
  79.3 19.3 %copy-start.1 = (bf16[1,2048,256]{2,1,0:T(8,128)(2,1)S(1)}, bf16[1,2048,256]{2,1,0:T(8,128)(2,1)}, u32[]{:S(2)}) copy-start(bf16[1,2048,256]{2,1,0:T(8,128)(2,1)} %param.12) | copy-start | bytes 3145732
  113.8 21.4 %copy-start.3 = (f32[1,504]{1,0:T(1,128)S(1)}, f32[1,504]{1,0:T(1,128)}, u32[]{:S(2)}) copy-start(f32[1,504]{1,0:T(1,128)} %affinity.1) | copy-start | bytes 6052
